TPU v7x, 256 devices: a whole 4x4x8 slice. The times are simulated.
256 devices in a mesh: sp: 128 (over z, y, x), tp: 2 (over core).
Axes of the slice: x: 4, y: 4, z: 8, core: 2. Of those that a mesh axis runs over, the one named last changes fastest.
Arguments:
- conv_value: bfloat16 [65536, 1536], P('sp', 'tp'), may hold values from -6 to 6
- conv_gate: bfloat16 [65536, 1536], P('sp', 'tp'), may hold values from -8 to 8
- conv_out: bfloat16 [65536, 1536], P('sp', 'tp'), may hold values from -40 to 40
- conv_taps: bfloat16 [31, 1536], P(None, 'tp'), may hold values from -1 to 1
- norm_gain: float32 [1536], P('tp'), may hold values from 0.1 to 1.9
- norm_shift: float32 [1536], P('tp'), may hold values from -3 to 3
- proj_weight: bfloat16 [2048, 1536], P(None, 'tp'), may hold values from -0.15625 to 0.15625
- out_grad: bfloat16 [65536, 2048], P('sp'), may hold values from -24 to 24
Outputs:
- grad_value: bfloat16 [65536, 1536], P('sp', 'tp')
- grad_gate: bfloat16 [65536, 1536], P('sp', 'tp')
- grad_taps: float32 [31, 1536], P(None, 'tp')
- grad_gain: float32 [1536], P('tp')
- grad_shift: float32 [1536], P('tp')
- grad_proj: float32 [2048, 1536], P('sp', 'tp')
All inputs are finite; a program needn't handle non-finite values.
Results may differ from a plain program's by a relative error of at most 0.005.
Values may be sent and summed in bfloat16 or wider, within the bound.
A program may use at most 64 MiB of HBM per device.

v0:
```python
import functools

import jax
import jax.numpy as jnp
from jax import lax
from jax.sharding import Mesh
from jax.sharding import PartitionSpec as P

SP = ("sp_0", "sp_1", "sp_2")


norm_eps = 1e-05


def own_rows_2(running, axes):
    for axis in axes:
        running = lax.psum_scatter(running, axis, scatter_dimension=0, tiled=True)
    return running


def shifted_2(block, axis, distance):
    devices = range(lax.axis_size(axis))
    route = [(i - distance, i) for i in devices if i - distance in devices]
    return lax.ppermute(block, axis, route)


def one_axis_at_a_time(array, axes):
    return functools.reduce(lax.psum, axes, array)


def project_rows(out_grad, active):
    return own_rows_2(
        lax.dot_general(
            out_grad, active, (((0,), (0,)), ((), ())), preferred_element_type=jnp.float32
        ),
        SP,
    )


def local(conv_value, conv_gate, conv_out, conv_taps, norm_gain, norm_shift, proj_weight, out_grad):
    seq_rows, chan_local = conv_value.shape
    tap_reach = conv_taps.shape[0] - 1
    chan_total = chan_local * lax.axis_size("tp")
    height = conv_out.astype(jnp.float32)
    center = lax.psum(jnp.sum(height, axis=1), "tp") / chan_total
    centered = height - center[:, None]
    variance = lax.psum(jnp.sum(centered * centered, axis=1), "tp") / chan_total
    inv_std = lax.rsqrt(variance + norm_eps)[:, None]
    normed = centered * inv_std
    shifted = normed * norm_gain + norm_shift
    sig_norm = jax.nn.sigmoid(shifted)
    active = (shifted * sig_norm).astype(jnp.bfloat16)
    act_grad = jnp.dot(out_grad, proj_weight, preferred_element_type=jnp.float32)
    norm_grad = act_grad * (sig_norm * (1.0 + shifted * (1.0 - sig_norm)))
    scaled = norm_grad * norm_gain
    grad_sum, grad_dot = lax.psum((jnp.sum(scaled, axis=1), jnp.sum(scaled * normed, axis=1)), "tp")
    height_grad = inv_std * (
        scaled - grad_sum[:, None] / chan_total - normed * (grad_dot[:, None] / chan_total)
    )
    sig_gate = jax.nn.sigmoid(conv_gate.astype(jnp.float32))
    value_float = conv_value.astype(jnp.float32)
    gated_rows = (value_float * sig_gate).astype(jnp.bfloat16)
    tap_values = conv_taps.astype(jnp.float32)
    earlier = shifted_2(gated_rows[seq_rows - tap_reach :], SP, 1)
    extended = jnp.concatenate([earlier, gated_rows], axis=0).astype(jnp.float32)
    padded_grad = jnp.pad(height_grad, ((tap_reach, tap_reach), (0, 0)))
    spill_rows = jnp.zeros((seq_rows + tap_reach, chan_local), jnp.float32)
    for tap_index in range(tap_reach + 1):
        begin = tap_reach - tap_index
        spill_rows = (
            spill_rows + tap_values[tap_index] * padded_grad[begin : begin + seq_rows + tap_reach]
        )
    returned = shifted_2(spill_rows[:tap_reach], SP, -1)
    gated_grad = spill_rows[tap_reach:] + jnp.pad(returned, ((seq_rows - tap_reach, 0), (0, 0)))
    tap_rows = jnp.stack(
        [
            jnp.sum(height_grad * extended[tap_index : tap_index + seq_rows], axis=0)
            for tap_index in range(tap_reach + 1)
        ]
    )
    gain_row = jnp.sum(norm_grad * normed, axis=0)
    shift_row = jnp.sum(norm_grad, axis=0)
    grad_taps, grad_gain, grad_shift = (
        one_axis_at_a_time(tap_rows, SP),
        one_axis_at_a_time(gain_row, SP),
        one_axis_at_a_time(shift_row, SP),
    )
    grad_value = (gated_grad * sig_gate).astype(jnp.bfloat16)
    grad_gate = (gated_grad * value_float * sig_gate * (1.0 - sig_gate)).astype(jnp.bfloat16)
    grad_proj = project_rows(out_grad, active)
    return (grad_value, grad_gate, grad_taps, grad_gain, grad_shift, grad_proj)


def solution(mesh):
    split = Mesh(mesh.devices.reshape(8, 4, 4, mesh.shape["tp"]), ("sp_0", "sp_1", "sp_2", "tp"))
    placed = (
        P(SP, "tp"),
        P(SP, "tp"),
        P(SP, "tp"),
        P(None, "tp"),
        P("tp"),
        P("tp"),
        P(None, "tp"),
        P(SP, None),
    )
    return jax.shard_map(
        local,
        mesh=split,
        in_specs=placed,
        out_specs=(P(SP, "tp"), P(SP, "tp"), P(None, "tp"), P("tp"), P("tp"), P(SP, "tp")),
        check_vma=False,
    )
```

profile of v0, /device:TPU:2, one launch (start us, length us, event | category | flops | bytes accessed | tf_op | source)
XLA Modules:
  0.0 349.0 jit_solution(18354876950033820677)
XLA Ops:
  7.2 0.0 copy-start
  7.2 0.0 copy-start.8
  7.2 0.0 copy-start.9
  7.2 0.0 all-reduce.10.cloned.1.call-start
  7.2 0.0 copy-start.2
  7.3 2.0 fusion.54
  9.2 0.0 copy-start.5
  9.2 0.9 copy-done.5
  10.1 3.4 collective-permute-start.1
  13.5 0.0 copy-done.2
  13.6 0.2 convert_reduce_fusion
  13.7 2.5 psum.91
  16.2 1.5 fusion.50
  17.7 2.5 psum.92
  20.2 0.0 copy-done
  20.2 0.0 copy-done.8
  20.2 0.0 copy-done.9
  20.2 5.4 %fusion.49 = (f32[768]{0:T(1024)S(1)}, f32[512]{0:T(512)S(1)}, f32[512]{0:T(512)S(1)}, f32[768]{0:T(1024)S(1)}, f32[512,768]{1,0:T(8,128)}) fusion(bf16[512,768]{1,0:T(8,128)(2,1)} %param.10, f32[512]{0:T(512)S(1)} %add_rsqrt_fusion, f32[512]{0:T(512)S(1)} %broadcast_multiply_fusion.2, f32[768]{0:T(1024)S(1)} %copy-done.8, f32[768]{0:T(1024)S(1)} %copy-done.9, ...), kind=kOutput, calls=%fused_computation.70 | convolution fusion | flops 1618474496 | bytes 7622656 | tf_op jit(solution)/shard_map/dot_general | solution.py:53
  25.6 2.4 all-reduce.5
  28.0 0.0 copy-start.3
  28.0 0.0 copy-start.6
  28.0 0.0 collective-permute-done.1
  28.0 1.4 maximum_convert_fusion
  29.5 0.0 copy-done.3
  29.5 0.4 copy-done.6
  29.9 4.8 %fusion.55 = (f32[768]{0:T(1024)S(1)}, f32[768]{0:T(1024)S(1)}, f32[768]{0:T(1024)S(1)}, f32[768]{0:T(1024)S(1)}, f32[768]{0:T(1024)S(1)}, /*index=5*/f32[768]{0...) fusion(f32[542,768]{1,0:T(8,128)S(1)} %maximum_convert_fusion, ...), kind=kLoop, calls=%fused_computation.77 | loop fusion | flops 17287680 | bytes 32310272 | tf_op jit(solution)/shard_map/reduce_sum | solution.py:77
  34.7 0.0 copy-start.1
  34.7 2.5 fusion.73
  37.3 0.0 copy-done.1
  37.6 2.6 stack.127
  40.2 0.0 all-reduce.10.cloned.1.call-update
  40.3 0.0 reduce-scatter.8.cloned.1.call-start
  40.3 6.6 %convolution_bitcast_fusion = f32[2048,768]{0,1:T(8,128)} fusion(bf16[512,2048]{1,0:T(8,128)(2,1)} %param.15, bf16[512,768]{1,0:T(8,128)(2,1)} %param.10, f32[768]{0:T(1024)S(1)} %copy-done.9, f32[768]{0:T(1024)S(1)} %copy-done.8, f32[512]{0:T(512)S(1)} %add_rsqrt_fusion, f32[512]{0:T(512)S(1)} %broadcast_multiply_fusion.2), kind=kOutput, calls=%fused_computation | convolution fusion | flops 1614544896 | bytes 9185280 | tf_op jit(solution)/shard_map/dot_general | solution.py:33
  46.9 0.0 reduce-scatter.8.cloned.1.call-update
  46.9 0.0 copy-start.7
  46.9 0.0 all-reduce.12.cloned.1.call-start
  47.0 68.5 %all-reduce.10.cloned.1.call-done = f32[31,768]{1,0:T(8,128)} async-done(((f32[31,768]{1,0:T(8,128)}), f32[31,768]{1,0:T(8,128)}) %all-reduce.10.cloned.1.call-update) | async-done | bytes 95248 | tf_op jit(solution)/shard_map/psum | solution.py:28
  115.5 0.0 all-reduce.12.cloned.1.call-update
  115.5 0.0 reduce-scatter.10.cloned.1.call-start
  115.6 75.7 %reduce-scatter.8.cloned.1.call-done = f32[256,768]{0,1:T(8,128)} async-done(((f32[2048,768]{0,1:T(8,128)}), f32[256,768]{0,1:T(8,128)}) %reduce-scatter.8.cloned.1.call-update) | async-done | bytes 786448 | tf_op jit(solution)/shard_map/reduce_scatter | solution.py:17
  191.3 2.3 copy.16
  193.5 0.0 reduce-scatter.10.cloned.1.call-update
  193.6 0.0 all-reduce.14.cloned.1.call-start
  193.6 0.0 copy-done.7
  193.6 0.1 slice_reduce_fusion.29
  193.8 0.2 slice_reduce_fusion.30
  193.9 44.8 %all-reduce.12.cloned.1.call-done = f32[31,768]{1,0:T(8,128)} async-done(((f32[31,768]{1,0:T(8,128)}), f32[31,768]{1,0:T(8,128)}) %all-reduce.12.cloned.1.call-update) | async-done | bytes 95248 | tf_op jit(solution)/shard_map/psum | solution.py:28
  238.7 0.0 all-reduce.14.cloned.1.call-update
  238.7 0.2 reduce-scatter.12.cloned.1.call-start
  238.9 25.3 %multiply_add_fusion = f32[542,768]{1,0:T(8,128)S(1)} fusion(f32[512,768]{1,0:T(8,128)} %copy-done.1, f32[768]{0:T(1024)S(1)} %get-tuple-element.54, f32[768]{0:T(1024)S(1)} %get-tuple-element.55, f32[768]{0:T(1024)S(1)} %get-tuple-element.56, f32[768]{0:T(1024)S(1)} %get-tuple-element.57, f32[768]{0:T(1024)S(1)} %get-tuple-element.58, ...), kind=kLoop, calls=%fused_computation.11 | loop fusion | flops 25391616 | bytes 3333120 | tf_op jit(solution)/shard_map/add | solution.py:71
  264.2 0.0 copy-start.4
  264.2 1.2 copy-done.4
  265.4 2.5 collective-permute-start
  267.9 17.7 %all-reduce.2 = (f32[768]{0:T(1024)S(1)}, f32[768]{0:T(1024)S(1)}) all-reduce(f32[768]{0:T(1024)S(1)} %get-tuple-element.49, f32[768]{0:T(1024)S(1)} %get-tuple-element.52), channel_id=1, replica_groups=mesh['sp_0'=8,'sp_1'=4,'sp_2'=4,'tp'=2] {'sp_0'}, use_global_device_ids=true, to_apply=%region_43.44 | all-reduce | flops 1536 | bytes 12288 | tf_op jit(solution)/shard_map/psum | solution.py:28
  285.6 9.4 %all-reduce.4 = (f32[768]{0:T(1024)S(1)}, f32[768]{0:T(1024)S(1)}) all-reduce(f32[768]{0:T(1024)S(1)} %get-tuple-element.84, f32[768]{0:T(1024)S(1)} %get-tuple-element.85), channel_id=1, replica_groups=mesh['sp_0'=8,'sp_1'=4,'sp_2'=4,'tp'=2] {'sp_1'}, use_global_device_ids=true, to_apply=%region_44.45 | all-reduce | flops 1536 | bytes 12288 | tf_op jit(solution)/shard_map/psum | solution.py:28
  295.0 11.7 %all-reduce.3 = (f32[768]{0:T(1024)}, f32[768]{0:T(1024)}) all-reduce(f32[768]{0:T(1024)S(1)} %get-tuple-element.88, f32[768]{0:T(1024)S(1)} %get-tuple-element.89), channel_id=1, replica_groups=mesh['sp_0'=8,'sp_1'=4,'sp_2'=4,'tp'=2] {'sp_2'}, use_global_device_ids=true, to_apply=%region_45.46 | all-reduce | flops 1536 | bytes 12288 | tf_op jit(solution)/shard_map/psum | solution.py:28
  306.7 0.0 reduce-scatter.10.cloned.1.call-done
  306.7 0.0 reduce-scatter.12.cloned.1.call-update
  306.7 0.0 collective-permute-done
  306.7 3.7 %fusion.53 = (bf16[512,768]{1,0:T(8,128)(2,1)}, bf16[512,768]{1,0:T(8,128)(2,1)}) fusion(bf16[512,768]{1,0:T(8,128)(2,1)} %param.8, f32[30,768]{1,0:T(8,128)S(1)} %collective-permute-done, f32[542,768]{1,0:T(8,128)} %copy-done.4, bf16[512,768]{1,0:T(8,128)(2,1)} %param.9), kind=kLoop, calls=%fused_computation.74 | loop fusion | flops 5111808 | bytes 4810752 | tf_op jit(solution)/shard_map/convert_element_type | solution.py:89
  310.5 4.1 %all-reduce.14.cloned.1.call-done = f32[31,768]{1,0:T(8,128)} async-done(((f32[31,768]{1,0:T(8,128)}), f32[31,768]{1,0:T(8,128)}) %all-reduce.14.cloned.1.call-update) | async-done | bytes 95248 | tf_op jit(solution)/shard_map/psum | solution.py:28
  314.6 26.0 %reduce-scatter.12.cloned.1.call-done = f32[16,768]{1,0:T(8,128)} async-done(((f32[64,768]{1,0:T(8,128)}), f32[16,768]{1,0:T(8,128)}) %reduce-scatter.12.cloned.1.call-update) | async-done | bytes 49168
  340.6 1.5 copy.23
  (37 shorter events, 0.2 us)
Async XLA Ops:
  7.2 13.0 %copy-start = (bf16[2048,768]{1,0:T(8,128)(2,1)S(1)}, bf16[2048,768]{1,0:T(8,128)(2,1)}, u32[]{:S(2)}) copy-start(bf16[2048,768]{1,0:T(8,128)(2,1)} %param.14) | copy-start | bytes 9437188
  7.2 13.0 %copy-start.8 = (f32[768]{0:T(1024)S(1)}, f32[768]{0:T(1024)}, u32[]{:S(2)}) copy-start(f32[768]{0:T(1024)} %param.12) | copy-start | bytes 9220
  7.2 13.0 %copy-start.9 = (f32[768]{0:T(1024)S(1)}, f32[768]{0:T(1024)}, u32[]{:S(2)}) copy-start(f32[768]{0:T(1024)} %param.13) | copy-start | bytes 9220
  7.2 108.3 %all-reduce.10.cloned.1.call-start = ((), (), s32[]{:S(2)}) async-start(), calls=%async_computation.3 | async-start | bytes 196608 | tf_op jit(solution)/shard_map/psum | solution.py:28
  7.2 6.3 %copy-start.2 = (bf16[512,768]{1,0:T(8,128)(2,1)S(1)}, bf16[512,768]{1,0:T(8,128)(2,1)}, u32[]{:S(2)}) copy-start(bf16[512,768]{1,0:T(8,128)(2,1)} %param.10) | copy-start | bytes 2359300
  9.2 0.9 copy-start.5
  10.1 17.9 %collective-permute-start.1 = (bf16[30,768]{1,0:T(8,128)(2,1)S(1)}, bf16[30,768]{1,0:T(8,128)(2,1)S(1)}, u32[]{:S(2)}, u32[]{:S(2)}) collective-permute-start(bf16[30,768]{1,0:T(8,128)(2,1)S(1)} %slice.417), channel_id=1, source_target_pairs={{0,2},{2,4},{4,6},{6,8},{8,10},{10,12},{12,14},{14,16},{16,18},{18... | collective-permute-start | bytes 138248 | tf_op jit(solution)/shard_map/ppermute | solution.py:24
  28.0 1.5 copy-start.3
  28.0 1.9 copy-start.6
  34.7 2.6 copy-start.1
  40.3 151.0 %reduce-scatter.8.cloned.1.call-start = ((), (), s32[]{:S(2)}) async-start(), calls=%async_computation.6 | async-start | bytes 7077888 | tf_op jit(solution)/shard_map/reduce_scatter | solution.py:17
  46.9 146.7 %copy-start.7 = (bf16[31,768]{1,0:T(8,128)(2,1)S(1)}, bf16[31,768]{1,0:T(8,128)(2,1)}, u32[]{:S(2)}) copy-start(bf16[31,768]{1,0:T(8,128)(2,1)} %param.11) | copy-start | bytes 142852
  46.9 191.8 %all-reduce.12.cloned.1.call-start = ((), (), s32[]{:S(2)}) async-start(), calls=%async_computation.4 | async-start | bytes 196608 | tf_op jit(solution)/shard_map/psum | solution.py:28
  115.5 191.2 %reduce-scatter.10.cloned.1.call-start = ((), (), s32[]{:S(2)}) async-start(), calls=%async_computation.7 | async-start | bytes 983040
  193.6 121.0 %all-reduce.14.cloned.1.call-start = ((), (), s32[]{:S(2)}) async-start(), calls=%async_computation.5 | async-start | bytes 196608 | tf_op jit(solution)/shard_map/psum | solution.py:28
  238.7 101.9 %reduce-scatter.12.cloned.1.call-start = ((), (), s32[]{:S(2)}) async-start(), calls=%async_computation.8 | async-start | bytes 245760
  264.2 1.2 copy-start.4
  265.4 41.3 %collective-permute-start = (f32[30,768]{1,0:T(8,128)S(1)}, f32[30,768]{1,0:T(8,128)S(1)}, u32[]{:S(2)}, u32[]{:S(2)}) collective-permute-start(f32[30,768]{1,0:T(8,128)S(1)} %slice.416), channel_id=1, source_target_pairs={{2,0},{4,2},{6,4},{8,6},{10,8},{12,10},{14,12},{16,14},{18,16},{20... | collective-permute-start | bytes 276488 | tf_op jit(solution)/shard_map/ppermute | solution.py:24
Sparse Core Ops, SparseCore 0:
  40.4 75.0 all-reduce.9
  118.1 73.1 reduce-scatter.7
  193.6 45.0 all-reduce.11
  241.7 25.6 reduce-scatter.9
  269.5 44.9 all-reduce.13
  317.5 23.0 reduce-scatter.11
where the time goes:
time: 351 us; the launch traced here: 349 us
  waiting for transfers between devices  219 us (62%)
  blocking collectives  46.2 us (13%)
  other arithmetic  41.4 us (12%)
  between operations  14.6 us (4%)
  matrix products  11.9 us (3%)
  local copies, waits for them, and re-layouts  9.34 us (3%)
  starting transfers between devices  6.28 us (2%)
    psum x3, waiting for transfers between devices, one_axis_at_a_time(): return functools.reduce(lax.psum, axes, array)  117 us
    reduce_scatter x1, waiting for transfers between devices, own_rows_2(): running = lax.psum_scatter(running, axis, scatter_dimension=0, tiled=True)  75.7 us
    psum x3, blocking collectives, one_axis_at_a_time(): return functools.reduce(lax.psum, axes, array)  38.8 us
    unnamed x8, waiting for transfers between devices  26.1 us
    add x1, other arithmetic, local(): spill_rows + tap_values[tap_index] * padded_grad[begin:begin + seq_rows +...  25.3 us
    reduce_sum x2, other arithmetic, local(): jnp.sum(height_grad * extended[tap_index:tap_index + seq_rows], axis=0)  7.32 us
  transfers between devices with their start and end apart: 8, of which 5 were waited for; matrix products, arithmetic and copies ran while one was open for 13% of the time, Pallas kernels for 0%

commit v1 on v0

v1 whole, which is shorter than its diff:
```python
import functools

import jax
import jax.numpy as jnp
from jax import lax
from jax.experimental import pallas as pl
from jax.experimental.pallas import tpu as pltpu
from jax.sharding import Mesh
from jax.sharding import PartitionSpec as P

MESH = pl.DeviceIdType.MESH
F32 = jnp.float32
BF16 = jnp.bfloat16
SP = ("z", "y", "x")
EPS = 1e-05
HALO = 32
LANE = 128
TILE = 32


class Slots:
    def __init__(self):
        self.used = 0

    def take(self, count):
        first = self.used
        self.used += count
        return first


def layout(nz, ny, nx):
    slots = Slots()
    plane = ny * nx
    return slots, {
        "stat": slots.take(1),
        "sums": slots.take(1),
        "gated": slots.take(1),
        "height": slots.take(1),
        "x1": slots.take(nx - 1),
        "y1": slots.take(ny - 1),
        "x2": slots.take(ny - 1),
        "y2": slots.take(nx - 1),
        "x3": slots.take(nz - 1),
        "y3": slots.take(nz - 1),
        "zr": slots.take(nz // 2),
        "zl": slots.take(nz // 2),
        "z2": slots.take(nx - 1),
        "z3": slots.take(ny - 1),
        "a1": slots.take(plane - 1),
        "a2": slots.take(nz),
        "a3": slots.take(plane - 1),
    }


def kernel(sizes, *refs):
    nz, ny, nx, rows, chan, depth, taps = sizes
    (cv_h, cg_h, co_h, taps_h, gain_h, shift_h, w_h, og_h, gv_o, gg_o, small_o, proj_o), rest = refs[:12], refs[12:]
    (co_v, og_v, w_v, cv_v, cg_v, taps_v, gain_v, shift_v, st_s, st_r, s2_s, s2_r, iv_v, sg_v, gt_v, nm_v, ds_v,
     act_v, ag_v, hg_v, gh_s, gh_r, hh_s, hh_r, px, py, pz, rx, ry, rzr, rzl, sx, sy, rx2, ry2, tx, ty, rx3, ry3,
     sz, rz2, tz, rz3, proj_v, sa, ra, fa, rza, fin, ag_a, small_v, gv_v, gg_v, in_sem, out_sem, ssem, rsem) = rest
    blocks = chan // LANE
    total = 2 * chan
    reach = taps - 1
    plane = ny * nx
    _, at = layout(nz, ny, nx)
    z, y, x, core = (lax.axis_index(a) for a in ("z", "y", "x", "tp"))
    place = y * nx + x
    line = z * plane + place
    count = nz * plane

    def where(index):
        return {"z": lax.div(index, plane), "y": lax.rem(lax.div(index, nx), ny), "x": lax.rem(index, nx)}

    after = where(lax.rem(line + 1, count))
    before = where(lax.rem(line + count - 1, count))
    other = {"tp": 1 - core}

    def along(axis, size, me, step):
        return {axis: lax.rem(me + step + size, size)}

    def in_plane(step):
        p = lax.rem(place + step, plane)
        return {"y": lax.div(p, nx), "x": lax.rem(p, nx)}

    def remote(src, dst, slot, target):
        return pltpu.make_async_remote_copy(
            src_ref=src, dst_ref=dst, send_sem=ssem.at[slot], recv_sem=rsem.at[slot],
            device_id=target, device_id_type=MESH)

    barrier = pltpu.get_barrier_semaphore()
    peers = [other, after, before]
    peers += [in_plane(o) for o in range(1, plane)]
    peers += [along("z", nz, z, o) for o in range(1, nz)]
    for peer in peers:
        pl.semaphore_signal(barrier, inc=1, device_id=peer, device_id_type=MESH)

    loads = {}
    for slot, (name, src, dst) in enumerate((
            ("co", co_h, co_v), ("gain", gain_h, gain_v), ("shift", shift_h, shift_v), ("cg", cg_h, cg_v),
            ("cv", cv_h, cv_v), ("og", og_h, og_v), ("w", w_h, w_v), ("taps", taps_h, taps_v))):
        loads[name] = pltpu.make_async_copy(src, dst, in_sem.at[slot])
        loads[name].start()

    lane = lax.broadcasted_iota(jnp.int32, (1, LANE), 1)
    first = lane < LANE // 2

    def lanes(b):
        return slice(b * LANE, (b + 1) * LANE)

    loads["co"].wait()

    def stats(i, carry):
        r = pl.ds(pl.multiple_of(i * 64, 64), 64)
        v = co_v[r, :].astype(F32)
        m = jnp.sum(v, axis=1, keepdims=True) * (1.0 / chan)
        d = v - m
        q = jnp.sum(d * d, axis=1, keepdims=True)
        st_s[r, :] = jnp.where(first, m, q)
        return carry

    lax.fori_loop(0, rows // 64, stats, 0)

    loads["cg"].wait()
    loads["cv"].wait()

    def gates(i, carry):
        r = pl.ds(pl.multiple_of(i * TILE, TILE), TILE)
        up = pl.ds(pl.multiple_of(i * TILE + HALO, TILE), TILE)
        for b in range(blocks):
            s = 0.5 * jnp.tanh(0.5 * cg_v[r, lanes(b)].astype(F32)) + 0.5
            sg_v[r, lanes(b)] = s
            gt_v[b, up, :] = (cv_v[r, lanes(b)].astype(F32) * s).astype(BF16).astype(F32)
        return carry

    lax.fori_loop(0, rows // TILE, gates, 0)
    for b in range(blocks):
        gh_s[:, lanes(b)] = gt_v[b, rows:rows + HALO, :].astype(BF16)

    pl.semaphore_wait(barrier, len(peers))
    stat_copy = remote(st_s, st_r, at["stat"], other)
    stat_copy.start()
    gated_copy = remote(gh_s, gh_r, at["gated"], after)
    gated_copy.start()

    loads["og"].wait()
    loads["w"].wait()

    def back(i, carry):
        r = pl.ds(pl.multiple_of(i * 128, 128), 128)
        ag_v[r, :] = jnp.dot(og_v[r, :], w_v[...], preferred_element_type=F32)
        return carry

    lax.fori_loop(0, rows // 128, back, 0)
    loads["gain"].wait()
    loads["shift"].wait()
    stat_copy.wait_recv()

    def norm(i, carry):
        r = pl.ds(pl.multiple_of(i * TILE, TILE), TILE)
        mine, theirs = st_s[r, :], st_r[r, :]
        m1, q1 = mine[:, 0:1], mine[:, 64:65]
        m2, q2 = theirs[:, 0:1], theirs[:, 64:65]
        gap = m1 - m2
        mean = 0.5 * (m1 + m2)
        inv = lax.rsqrt((q1 + q2 + gap * gap * (chan / 2)) * (1.0 / total) + EPS)
        inv = jnp.broadcast_to(inv, (TILE, LANE))
        mean = jnp.broadcast_to(mean, (TILE, LANE))
        iv_v[r, :] = inv
        for b in range(blocks):
            n = (co_v[r, lanes(b)].astype(F32) - mean) * inv
            s = n * gain_v[:, lanes(b)] + shift_v[:, lanes(b)]
            sig = 0.5 * jnp.tanh(0.5 * s) + 0.5
            a = s * sig
            act_v[r, lanes(b)] = a.astype(BF16)
            nm_v[r, lanes(b)] = n
            ds_v[r, lanes(b)] = sig + a * (1.0 - sig)
        return carry

    lax.fori_loop(0, rows // TILE, norm, 0)

    third = chan // 3
    span = plane * 16
    half = ny // 2

    def z_first(step_slot, src_z, part, direction):
        buf, base = (rzr, at["zr"]) if direction > 0 else (rzl, at["zl"])
        src, dst = pz.at[src_z], buf.at[step_slot]
        if part is not None:
            src, dst = src.at[part], dst.at[part]
        return remote(src, dst, base + step_slot, along("z", nz, z, direction))

    upper, lower = pl.ds(0, half), pl.ds(half, half)

    def project(k, carry):
        away = nz // 2 - lax.div(k + 1, 2)
        sign = 2 * lax.rem(k, 2) - 1
        zz = lax.rem(z + sign * away + nz, nz)
        cols = pl.ds(pl.multiple_of(zz * span, span), span)
        block = lax.dot_general(og_v[:, cols], act_v[...], (((0,), (0,)), ((), ())), preferred_element_type=F32)
        block = block.astype(BF16)
        for yy in range(ny):
            for xx in range(nx):
                part = slice((yy * nx + xx) * 16, (yy * nx + xx) * 16 + 16)
                px[xx, zz, yy] = block[part, 0:third]
                py[yy, zz, xx] = block[part, third:2 * third]
                pz[zz, yy, xx] = block[part, 2 * third:]
        for o in range(1, nx):
            peer = along("x", nx, x, o)
            remote(px.at[peer["x"], zz], rx.at[o - 1, zz], at["x1"] + o - 1, peer).start()
        for o in range(1, ny):
            peer = along("y", ny, y, o)
            remote(py.at[peer["y"], zz], ry.at[o - 1, zz], at["y1"] + o - 1, peer).start()

        @pl.when(k == 0)
        def _():
            z_first(0, zz, upper, 1).start()
            z_first(0, zz, lower, -1).start()

        return carry

    lax.fori_loop(0, nz, project, 0)

    def grads(i, carry):
        r = pl.ds(pl.multiple_of(i * TILE, TILE), TILE)
        carry = list(carry)
        row_sum = jnp.zeros((TILE, LANE), F32)
        row_dot = jnp.zeros((TILE, LANE), F32)
        for b in range(blocks):
            g = ag_v[r, lanes(b)] * ds_v[r, lanes(b)]
            n = nm_v[r, lanes(b)]
            gn = g * n
            carry[b] = carry[b] + jnp.sum(gn.reshape(TILE // 8, 8, LANE), axis=0)
            carry[blocks + b] = carry[blocks + b] + jnp.sum(g.reshape(TILE // 8, 8, LANE), axis=0)
            gain = gain_v[:, lanes(b)]
            s = g * gain
            ag_v[r, lanes(b)] = s
            row_sum = row_sum + s
            row_dot = row_dot + gn * gain
        sums = jnp.sum(row_sum, axis=1, keepdims=True)
        dots = jnp.sum(row_dot, axis=1, keepdims=True)
        s2_s[r, :] = jnp.where(first, sums, dots)
        return tuple(carry)

    partial = lax.fori_loop(0, rows // TILE, grads, tuple(jnp.zeros((8, LANE), F32) for _ in range(2 * blocks)))
    sums_copy = remote(s2_s, s2_r, at["sums"], other)
    sums_copy.start()

    z_recv = []

    def z_step(step):
        for direction in (1, -1):
            dest = lax.rem(z + direction * (nz // 2 - step) + nz, nz)
            part = None
            if step == 1:
                part = upper if direction > 0 else lower
            z_first(step - 1, dest, part, direction).wait_recv()
            buf = rzr if direction > 0 else rzl
            ys = range(ny) if step > 1 else (range(half) if direction > 0 else range(half, ny))
            for yy in ys:
                pz[dest, yy] = (pz[dest, yy].astype(F32) + buf[step - 1, yy].astype(F32)).astype(BF16)
            z_first(step, dest, None, direction).start()

    z_step(1)

    gated_copy.wait_recv()
    for b in range(blocks):
        head = gh_r[:, lanes(b)].astype(F32)
        gt_v[b, 0:HALO, :] = jnp.where(line == 0, 0.0, head)

    sums_copy.wait_recv()

    def height(i, carry):
        r = pl.ds(pl.multiple_of(i * TILE, TILE), TILE)
        both = (s2_s[r, :] + s2_r[r, :]) * (1.0 / total)
        sums = jnp.broadcast_to(both[:, 0:1], (TILE, LANE))
        dots = jnp.broadcast_to(both[:, 64:65], (TILE, LANE))
        inv = iv_v[r, :]
        for b in range(blocks):
            hg_v[b, r, :] = inv * (ag_v[r, lanes(b)] - sums - nm_v[r, lanes(b)] * dots)
        return carry

    lax.fori_loop(0, rows // TILE, height, 0)
    for b in range(blocks):
        hh_s[:, lanes(b)] = hg_v[b, 0:HALO, :].astype(BF16)
    height_copy = remote(hh_s, hh_r, at["height"], before)
    height_copy.start()

    small_rows = (taps + 2 + 7) // 8
    flat = sa.shape[0] * sa.shape[1]

    def tap_block(b):
        def step(t, acc):
            base = t * 8
            h = hg_v[b, pl.ds(pl.multiple_of(base, 8), 8), :]
            return tuple(
                acc[j] + h * gt_v[b, pl.ds(base + (HALO - reach) + j, 8), :] for j in range(taps))

        acc = lax.fori_loop(0, rows // 8, step, tuple(jnp.zeros((8, LANE), F32) for _ in range(taps)))
        acc = list(acc) + [partial[b], partial[blocks + b]]
        lines = [jnp.sum(a, axis=0, keepdims=True) for a in acc]
        lines += [jnp.zeros((1, LANE), F32)] * (small_rows * 8 - len(lines))
        for t in range(small_rows):
            tile = b * small_rows + t
            sa[tile // 2, tile % 2] = jnp.concatenate(lines[t * 8:t * 8 + 8], axis=0)

    for b in range(blocks):
        tap_block(b)
        if b == 1:
            z_step(2)
        if b == 4:
            z_step(3)
    for tile in range(blocks * small_rows, flat):
        sa[tile // 2, tile % 2] = jnp.zeros((8, LANE), F32)
    for o in range(1, plane):
        remote(sa.at[lax.rem(place + o, plane)], ra.at[o - 1], at["a1"] + o - 1, in_plane(o)).start()

    def gather_x(wide, me, got, out, name, axis, size, own_axis_size):
        for o in range(1, own_axis_size):
            remote(wide.at[me], got.at[o - 1], at[name + "1"] + o - 1, other).wait_recv()

        def step(zz, carry):
            v = wide[me, zz].astype(F32)
            for o in range(own_axis_size - 1):
                v = v + got[o, zz].astype(F32)
            v = v.astype(BF16)
            for w in range(size):
                out[w, zz] = v[w]
            return carry

        lax.fori_loop(0, nz, step, 0)

    gather_x(px, x, rx, sx, "x", "y", ny, nx)
    for o in range(1, ny):
        peer = along("y", ny, y, o)
        remote(sx.at[peer["y"]], rx2.at[o - 1], at["x2"] + o - 1, peer).start()
    gather_x(py, y, ry, sy, "y", "x", nx, ny)
    for o in range(1, nx):
        peer = along("x", nx, x, o)
        remote(sy.at[peer["x"]], ry2.at[o - 1], at["y2"] + o - 1, peer).start()

    def z_done():
        z_first(nz // 2 - 1, z, None, 1).wait_recv()
        z_first(nz // 2 - 1, z, None, -1).wait_recv()
        for yy in range(ny):
            v = pz[z, yy].astype(F32) + rzr[nz // 2 - 1, yy].astype(F32) + rzl[nz // 2 - 1, yy].astype(F32)
            v = v.astype(BF16)
            for xx in range(nx):
                sz[xx, yy] = v[xx]
        for o in range(1, nx):
            peer = along("x", nx, x, o)
            remote(sz.at[peer["x"]], rz2.at[o - 1], at["z2"] + o - 1, peer).start()

    def small_plane():
        for o in range(1, plane):
            remote(sa.at[0], ra.at[o - 1], at["a1"] + o - 1, in_plane(o)).wait_recv()
        v = sa[place]
        for o in range(plane - 1):
            v = v + ra[o]
        fa[...] = v
        rza[z] = v
        for o in range(1, nz):
            remote(fa, rza.at[z], at["a2"] + z, along("z", nz, z, o)).start()

    def xy_third(own, me, got, out, last, name, size):
        for o in range(1, size):
            remote(own.at[0], got.at[o - 1], at[name + "2"] + o - 1, other).wait_recv()
        v = own[me].astype(F32)
        for o in range(size - 1):
            v = v + got[o].astype(F32)
        out[...] = v.astype(BF16)
        for o in range(1, nz):
            peer = along("z", nz, z, o)
            remote(out.at[peer["z"]], last.at[o - 1], at[name + "3"] + o - 1, peer).start()

    def z_third():
        for o in range(1, nx):
            remote(sz.at[0], rz2.at[o - 1], at["z2"] + o - 1, other).wait_recv()
        v = sz[x].astype(F32)
        for o in range(nx - 1):
            v = v + rz2[o].astype(F32)
        tz[...] = v.astype(BF16)
        for o in range(1, ny):
            peer = along("y", ny, y, o)
            remote(tz.at[peer["y"]], rz3.at[o - 1], at["z3"] + o - 1, peer).start()

    def small_line():
        for o in range(1, nz):
            zz = lax.rem(z + o, nz)
            remote(fa, rza.at[zz], at["a2"] + zz, other).wait_recv()
        v = rza[0]
        for zz in range(1, nz):
            v = v + rza[zz]
        fin[...] = v
        ag_a[place] = v
        for o in range(1, plane):
            remote(fin, ag_a.at[place], at["a3"] + o - 1, in_plane(o)).start()

    height_copy.wait_recv()
    for b in range(blocks):
        tail = hh_r[:, lanes(b)].astype(F32)
        hg_v[b, rows:rows + HALO, :] = jnp.where(line == count - 1, 0.0, tail)

    loads["taps"].wait()

    def gated_block(b):
        lines = taps_v[:, lanes(b)].astype(F32)
        spread = [jnp.broadcast_to(lines[j:j + 1, :], (8, LANE)) for j in range(taps)]

        def step(t, carry):
            base = t * 16
            r = pl.ds(pl.multiple_of(base, 16), 16)
            pieces = []
            for u in range(2):
                acc = None
                for j in range(taps):
                    term = spread[j] * hg_v[b, pl.ds(base + 8 * u + reach - j, 8), :]
                    acc = term if acc is None else acc + term
                pieces.append(acc)
            g = jnp.concatenate(pieces, axis=0)
            s = sg_v[r, lanes(b)]
            gs = g * s
            gv_v[r, lanes(b)] = gs.astype(BF16)
            gg_v[r, lanes(b)] = (gs * cv_v[r, lanes(b)].astype(F32) * (1.0 - s)).astype(BF16)
            return carry

        lax.fori_loop(0, rows // 16, step, 0)

    outs = []
    for b in range(blocks):
        gated_block(b)
        if b == 0:
            z_done()
        if b == 1:
            xy_third(sx, y, rx2, tx, rx3, "x", ny)
            xy_third(sy, x, ry2, ty, ry3, "y", nx)
        if b == 2:
            small_plane()
        if b == 3:
            z_third()
        if b == 5:
            small_line()

    outs.append(pltpu.make_async_copy(gv_v, gv_o, out_sem.at[0]))
    outs.append(pltpu.make_async_copy(gg_v, gg_o, out_sem.at[1]))
    for c in outs:
        c.start()

    for buf, own, last, name in ((0, tx, rx3, "x3"), (1, ty, ry3, "y3")):
        for o in range(1, nz):
            remote(own.at[0], last.at[o - 1], at[name] + o - 1, other).wait_recv()
        v = own[z].astype(F32)
        for o in range(nz - 1):
            v = v + last[o].astype(F32)
        proj_v[:, buf * third:(buf + 1) * third] = v
    for o in range(1, ny):
        remote(tz.at[0], rz3.at[o - 1], at["z3"] + o - 1, other).wait_recv()
    v = tz[y].astype(F32)
    for o in range(ny - 1):
        v = v + rz3[o].astype(F32)
    proj_v[:, 2 * third:] = v
    outs.append(pltpu.make_async_copy(proj_v, proj_o, out_sem.at[2]))
    outs[-1].start()

    for o in range(1, plane):
        p = lax.rem(place - o + plane, plane)
        remote(fin, ag_a.at[p], at["a3"] + o - 1, other).wait_recv()
    for b in range(blocks):
        for t in range(small_rows):
            tile = b * small_rows + t
            small_v[t * 8:t * 8 + 8, lanes(b)] = ag_a[tile // 2, tile % 2]
    outs.append(pltpu.make_async_copy(small_v, small_o, out_sem.at[3]))
    outs[-1].start()

    stat_copy.wait_send()
    gated_copy.wait_send()
    sums_copy.wait_send()
    height_copy.wait_send()
    for o in range(nx - 1):
        remote(px.at[0], rx.at[o], at["x1"] + o, other).wait_send()
        remote(sy.at[0], ry2.at[o], at["y2"] + o, other).wait_send()
        remote(sz.at[0], rz2.at[o], at["z2"] + o, other).wait_send()
    for o in range(ny - 1):
        remote(py.at[0], ry.at[o], at["y1"] + o, other).wait_send()
        remote(sx.at[0], rx2.at[o], at["x2"] + o, other).wait_send()
        remote(tz.at[0], rz3.at[o], at["z3"] + o, other).wait_send()
    for o in range(nz - 1):
        remote(tx.at[0], rx3.at[o], at["x3"] + o, other).wait_send()
        remote(ty.at[0], ry3.at[o], at["y3"] + o, other).wait_send()
    for step in range(nz // 2):
        z_first(step, z, upper if step == 0 else None, 1).wait_send()
        z_first(step, z, lower if step == 0 else None, -1).wait_send()
    for o in range(plane - 1):
        remote(sa.at[0], ra.at[o], at["a1"] + o, other).wait_send()
        remote(fin, ag_a.at[0], at["a3"] + o, other).wait_send()
    for o in range(1, nz):
        remote(fa, rza.at[z], at["a2"] + z, other).wait_send()
    for c in outs:
        c.wait()


def local(conv_value, conv_gate, conv_out, conv_taps, norm_gain, norm_shift, proj_weight, out_grad):
    nz, ny, nx = (lax.axis_size(a) for a in SP)
    rows, chan = conv_value.shape
    depth = out_grad.shape[1]
    taps = conv_taps.shape[0]
    blocks = chan // LANE
    third = chan // 3
    plane = ny * nx
    slots, _ = layout(nz, ny, nx)
    vm = pltpu.VMEM
    small_rows = (taps + 2 + 7) // 8 * 8
    per = -(-blocks * small_rows // 8 // plane)
    scratch = [
        vm((rows, chan), BF16), vm((rows, depth), BF16), vm((depth, chan), BF16), vm((rows, chan), BF16),
        vm((rows, chan), BF16), vm((taps, chan), BF16), vm((1, chan), F32), vm((1, chan), F32),
        vm((rows, LANE), F32), vm((rows, LANE), F32), vm((rows, LANE), F32), vm((rows, LANE), F32),
        vm((rows, LANE), F32), vm((rows, chan), F32), vm((blocks, rows + HALO, LANE), F32), vm((rows, chan), F32),
        vm((rows, chan), F32), vm((rows, chan), BF16), vm((rows, chan), F32), vm((blocks, rows + HALO, LANE), F32),
        vm((HALO, chan), BF16), vm((HALO, chan), BF16), vm((HALO, chan), BF16), vm((HALO, chan), BF16),
        vm((nx, nz, ny, 16, third), BF16), vm((ny, nz, nx, 16, third), BF16), vm((nz, ny, nx, 16, third), BF16),
        vm((nx - 1, nz, ny, 16, third), BF16), vm((ny - 1, nz, nx, 16, third), BF16),
        vm((nz // 2, ny, nx, 16, third), BF16), vm((nz // 2, ny, nx, 16, third), BF16),
        vm((ny, nz, 16, third), BF16), vm((nx, nz, 16, third), BF16),
        vm((ny - 1, nz, 16, third), BF16), vm((nx - 1, nz, 16, third), BF16),
        vm((nz, 16, third), BF16), vm((nz, 16, third), BF16),
        vm((nz - 1, 16, third), BF16), vm((nz - 1, 16, third), BF16),
        vm((nx, ny, 16, third), BF16), vm((nx - 1, ny, 16, third), BF16),
        vm((ny, 16, third), BF16), vm((ny - 1, 16, third), BF16),
        vm((16, chan), F32),
        vm((plane, per, 8, LANE), F32), vm((plane - 1, per, 8, LANE), F32), vm((per, 8, LANE), F32),
        vm((nz, per, 8, LANE), F32), vm((per, 8, LANE), F32), vm((plane, per, 8, LANE), F32),
        vm((small_rows, chan), F32), vm((rows, chan), BF16), vm((rows, chan), BF16),
        pltpu.SemaphoreType.DMA((8,)), pltpu.SemaphoreType.DMA((4,)),
        pltpu.SemaphoreType.DMA((slots.used,)), pltpu.SemaphoreType.DMA((slots.used,)),
    ]
    anywhere = pl.BlockSpec(memory_space=pl.ANY)
    grad_value, grad_gate, small, grad_proj = pl.pallas_call(
        functools.partial(kernel, (nz, ny, nx, rows, chan, depth, taps)),
        out_shape=(
            jax.ShapeDtypeStruct((rows, chan), BF16),
            jax.ShapeDtypeStruct((rows, chan), BF16),
            jax.ShapeDtypeStruct((small_rows, chan), F32),
            jax.ShapeDtypeStruct((16, chan), F32),
        ),
        in_specs=[anywhere] * 8,
        out_specs=(anywhere,) * 4,
        scratch_shapes=scratch,
        compiler_params=pltpu.CompilerParams(
            collective_id=0, has_side_effects=True, vmem_limit_bytes=62 * 1024 * 1024),
        name="module_backward",
    )(conv_value, conv_gate, conv_out, conv_taps, norm_gain.reshape(1, chan), norm_shift.reshape(1, chan),
      proj_weight, out_grad)
    return grad_value, grad_gate, small[:taps], small[taps], small[taps + 1], grad_proj


def solution(mesh):
    split = Mesh(mesh.devices.reshape(8, 4, 4, mesh.shape["tp"]), (*SP, "tp"))
    placed = (
        P(SP, "tp"), P(SP, "tp"), P(SP, "tp"), P(None, "tp"), P("tp"), P("tp"), P(None, "tp"), P(SP, None),
    )
    return jax.shard_map(
        local,
        mesh=split,
        in_specs=placed,
        out_specs=(P(SP, "tp"), P(SP, "tp"), P(None, "tp"), P("tp"), P("tp"), P(SP, "tp")),
        check_vma=False,
    )
```

time: 351 us -> 64 us (0.18)
  waiting for transfers between devices: 219 us -> 0 us
  Pallas kernels: 0 us -> 52.8 us
  blocking collectives: 46.2 us -> 0 us
  other arithmetic: 41.4 us -> 0 us
  between operations: 14.6 us -> 0.65 us
  matrix products: 11.9 us -> 0 us
  starting transfers between devices: 6.28 us -> 0 us
    psum x3 -> x0, waiting for transfers between devices: 117 us -> none  [one_axis_at_a_time(): return functools.reduce(lax.psum, axes, array)]
    reduce_scatter x1 -> x0, waiting for transfers between devices: 75.7 us -> none  [own_rows_2(): running = lax.psum_scatter(running, axis, scatter_dimension=0, tiled=True)]
    pallas_call x0 -> x1, Pallas kernels: none -> 52.8 us  [local(): pl.pallas_call(functools.partial(kernel, (nz, ny, nx, rows, chan, depth,...]
    psum x6 -> x0, blocking collectives: 46.2 us -> none  [the longest x3 38.8 us: one_axis_at_a_time(): return functools.reduce(lax.psum, axes, array)]
    unnamed x8 -> x0, waiting for transfers between devices: 26.1 us -> none
    add x1 -> x0, other arithmetic: 25.3 us -> none  [local(): spill_rows + tap_values[tap_index] * padded_grad[begin:begin + seq_rows +...]
    dot_general x2 -> x0, matrix products: 11.9 us -> none  [the longest x1 6.56 us: project_rows(): lax.dot_general(out_grad, active, (((0,), (0,)), ((), ())), preferred_ele...]
    reduce_sum x4 -> x0, other arithmetic: 8.99 us -> none  [the longest x2 7.32 us: local(): jnp.sum(height_grad * extended[tap_index:tap_index + seq_rows], axis=0)]
  transfers between devices with their start and end apart: 8 -> 0, of which waited for: 5 -> 0; matrix products, arithmetic and copies ran while one was open for 13% -> 0% of each run, Pallas kernels for 0% -> 0%
where the time goes in v1:
time: 64 us; the launch traced here: 63.7 us
  Pallas kernels  52.8 us (82%)
  local copies, waits for them, and re-layouts  10.2 us (16%)
  between operations  0.65 us (1%)
    pallas_call x1, Pallas kernels, local(): pl.pallas_call(functools.partial(kernel, (nz, ny, nx, rows, chan, depth,...  52.8 us
    unnamed x5, local copies, waits for them, and re-layouts  4.75 us
    slice x1, local copies, waits for them, and re-layouts, local(): small[:taps]  1.54 us
    slice x1, local copies, waits for them, and re-layouts, local(): small[taps + 1]  1.38 us

profile of v1, /device:TPU:2, one launch (start us, length us, event | category | flops | bytes accessed | tf_op | source)
XLA Modules:
  0.0 63.7 jit_solution(8029729485507317472)
XLA Ops:
  0.6 1.3 %reshape.18.refs_4_ = f32[1,768]{1,0:T(1,128)} reshape(f32[768]{0:T(1024)} %param.12) | data formatting | bytes 6144 | tf_op jit(solution)/shard_map/reshape | solution.py:551
  1.9 1.3 %reshape.19.refs_5_ = f32[1,768]{1,0:T(1,128)} reshape(f32[768]{0:T(1024)} %param.13) | data formatting | bytes 6144 | tf_op jit(solution)/shard_map/reshape | solution.py:551
  3.2 52.8 %module_backward.1 = (bf16[512,768]{1,0:T(8,128)(2,1)}, bf16[512,768]{1,0:T(8,128)(2,1)}, f32[40,768]{1,0:T(8,128)}, f32[16,768]{1,0:T(8,128)}) custom-call(bf16[512,768]{1,0:T(8,128)(2,1)} %refs_0_.1, bf16[512,768]{1,0:T(8,128)(2,1)} %refs_1_.1, bf16[512,768]{1,0:T(8,128)(2,1)} %refs_2_.1, bf16[31,768]{1,0:T(8,128)(2,1)} %refs_3_.1, ...), custom_call_target="tpu_custom_call" | custom-call | tf_op jit(solution)/shard_map/module_backward/pallas_call | solution.py:537
  56.0 0.0 copy-start
  56.0 1.4 %slice_reduce_fusion = (f32[768]{0:T(1024)}, f32[768]{0:T(1024)}) fusion(f32[40,768]{1,0:T(8,128)} %get-tuple-element.12), kind=kLoop, calls=%fused_computation | loop fusion | bytes 12288 | tf_op jit(solution)/shard_map/slice | solution.py:553
  57.4 1.5 %slice.9 = f32[31,768]{1,0:T(8,128)} slice(f32[40,768]{1,0:T(8,128)} %get-tuple-element.12), slice={[0:31], [0:768]} | slice | bytes 190464 | tf_op jit(solution)/shard_map/slice | solution.py:553
  58.9 2.1 %copy.17 = bf16[512,768]{1,0:T(8,128)(2,1)} copy(bf16[512,768]{1,0:T(8,128)(2,1)} %get-tuple-element.22) | data formatting | bytes 1572864
  61.0 2.1 %copy.18 = bf16[512,768]{1,0:T(8,128)(2,1)} copy(bf16[512,768]{1,0:T(8,128)(2,1)} %get-tuple-element.23) | data formatting | bytes 1572864
  63.1 0.0 copy-done
  63.1 0.6 copy.19
Async XLA Ops:
  56.0 7.1 %copy-start = (f32[16,768]{1,0:T(8,128)S(1)}, f32[16,768]{1,0:T(8,128)}, u32[]{:S(2)}) copy-start(f32[16,768]{1,0:T(8,128)} %get-tuple-element.27) | copy-start | bytes 147460

commit v2 on v1

v2 whole, which is shorter than its diff:
```python
import functools

import jax
import jax.numpy as jnp
from jax import lax
from jax.experimental import pallas as pl
from jax.experimental.pallas import tpu as pltpu
from jax.sharding import Mesh
from jax.sharding import PartitionSpec as P

MESH = pl.DeviceIdType.MESH
F32 = jnp.float32
BF16 = jnp.bfloat16
SP = ("z", "y", "x")
EPS = 1e-05
HALO = 32
LANE = 128
TILE = 32
GROUP = 4


class Slots:
    def __init__(self):
        self.used = 0

    def take(self, count):
        first = self.used
        self.used += count
        return first


def layout(nz, ny, nx):
    slots = Slots()
    plane = ny * nx
    return slots, {
        "stat": slots.take(1),
        "sums": slots.take(1),
        "gated": slots.take(1),
        "height": slots.take(1),
        "x1": slots.take(2 * (nx - 1)),
        "y1": slots.take(2 * (ny - 1)),
        "x2": slots.take(2 * (ny - 1)),
        "y2": slots.take(2 * (nx - 1)),
        "x3": slots.take(nz - 1),
        "y3": slots.take(nz - 1),
        "zr": slots.take(nz),
        "zl": slots.take(nz),
        "z2": slots.take(nx - 1),
        "z3": slots.take(ny - 1),
        "a1": slots.take(plane - 1),
        "a2": slots.take(nz),
        "a3": slots.take(plane - 1),
    }


def kernel(sizes, *refs):
    nz, ny, nx, rows, chan, depth, taps = sizes
    cv_h, cg_h, co_h, taps_h, gain_h, shift_h, w_h, og_h, gv_v, gg_v, taps_o, gain_o, shift_o, proj_v = refs[:14]
    (co_v, og_v, w_v, cv_v, cg_v, taps_v, gain_v, shift_v, st_s, st_r, s2_s, s2_r, iv_v, sg_v, gt_v, nm_v, ds_v,
     act_v, ag_v, hg_v, gh_s, gh_r, hh_s, hh_r, px, py, pz, rx, ry, rzr, rzl, sx, sy, rx2, ry2, tx, ty, rx3, ry3,
     sz, rz2, tz, rz3, sa, ra, fa, rza, fin, ag_a, in_sem, ssem, rsem) = refs[14:]
    blocks = chan // LANE
    total = 2 * chan
    reach = taps - 1
    plane = ny * nx
    _, at = layout(nz, ny, nx)
    z, y, x, core = (lax.axis_index(a) for a in ("z", "y", "x", "tp"))
    place = y * nx + x
    line = z * plane + place
    count = nz * plane

    def where(index):
        return {"z": lax.div(index, plane), "y": lax.rem(lax.div(index, nx), ny), "x": lax.rem(index, nx)}

    after = where(lax.rem(line + 1, count))
    before = where(lax.rem(line + count - 1, count))
    other = {"tp": 1 - core}

    def along(axis, size, me, step):
        return {axis: lax.rem(me + step + size, size)}

    def in_plane(step):
        p = lax.rem(place + step, plane)
        return {"y": lax.div(p, nx), "x": lax.rem(p, nx)}

    def remote(src, dst, slot, target):
        return pltpu.make_async_remote_copy(
            src_ref=src, dst_ref=dst, send_sem=ssem.at[slot], recv_sem=rsem.at[slot],
            device_id=target, device_id_type=MESH)

    loads = {}
    for slot, (name, src, dst) in enumerate((
            ("co", co_h, co_v), ("gain", gain_h, gain_v), ("shift", shift_h, shift_v), ("cg", cg_h, cg_v),
            ("cv", cv_h, cv_v), ("og", og_h, og_v), ("w", w_h, w_v), ("taps", taps_h, taps_v))):
        loads[name] = pltpu.make_async_copy(src, dst, in_sem.at[slot])
        loads[name].start()

    barrier = pltpu.get_barrier_semaphore()
    peers = [other, after, before]
    peers += [in_plane(o) for o in range(1, plane)]
    peers += [along("z", nz, z, o) for o in range(1, nz)]
    for peer in peers:
        pl.semaphore_signal(barrier, inc=1, device_id=peer, device_id_type=MESH)

    def lanes(b):
        return slice(b * LANE, (b + 1) * LANE)

    loads["co"].wait()

    wide = rows // 2

    def means(i, carry):
        for u in range(wide // 64):
            r = pl.ds(pl.multiple_of(i * wide + u * 64, 64), 64)
            m = jnp.sum(co_v[r, :].astype(F32), axis=1, keepdims=True) * (1.0 / chan)
            st_s[0, r, :] = jnp.broadcast_to(m, (64, LANE))
        return carry

    lax.fori_loop(0, 2, means, 0)

    def spreads(i, carry):
        for u in range(wide // 64):
            r = pl.ds(pl.multiple_of(i * wide + u * 64, 64), 64)
            m = st_s[0, r, :]
            q = jnp.zeros((64, LANE), F32)
            for b in range(blocks):
                d = co_v[r, lanes(b)].astype(F32) - m
                q = q + d * d
            st_s[1, r, :] = jnp.broadcast_to(jnp.sum(q, axis=1, keepdims=True), (64, LANE))
        return carry

    lax.fori_loop(0, 2, spreads, 0)

    loads["cg"].wait()
    loads["cv"].wait()

    def gates(i, carry):
        r = pl.ds(pl.multiple_of(i * TILE, TILE), TILE)
        up = pl.ds(pl.multiple_of(i * TILE + HALO, TILE), TILE)
        for b in range(blocks):
            s = 0.5 * jnp.tanh(0.5 * cg_v[r, lanes(b)].astype(F32)) + 0.5
            sg_v[r, lanes(b)] = s
            gt_v[b, up, :] = (cv_v[r, lanes(b)].astype(F32) * s).astype(BF16).astype(F32)
        return carry

    lax.fori_loop(0, rows // TILE, gates, 0)
    for b in range(blocks):
        gh_s[:, lanes(b)] = gt_v[b, rows:rows + HALO, :].astype(BF16)

    pl.semaphore_wait(barrier, len(peers))
    stat_copy = remote(st_s, st_r, at["stat"], other)
    stat_copy.start()
    gated_copy = remote(gh_s, gh_r, at["gated"], after)
    gated_copy.start()

    loads["gain"].wait()
    loads["shift"].wait()
    stat_copy.wait_recv()

    def norm(i, carry):
        r = pl.ds(pl.multiple_of(i * TILE, TILE), TILE)
        m1, m2 = st_s[0, r, :], st_r[0, r, :]
        gap = m1 - m2
        mean = 0.5 * (m1 + m2)
        inv = lax.rsqrt((st_s[1, r, :] + st_r[1, r, :] + gap * gap * (chan / 2)) * (1.0 / total) + EPS)
        iv_v[r, :] = inv
        for b in range(blocks):
            n = (co_v[r, lanes(b)].astype(F32) - mean) * inv
            s = n * gain_v[lanes(b)].reshape(1, LANE) + shift_v[lanes(b)].reshape(1, LANE)
            sig = 0.5 * jnp.tanh(0.5 * s) + 0.5
            a = s * sig
            act_v[r, lanes(b)] = a.astype(BF16)
            nm_v[r, lanes(b)] = n
            ds_v[r, lanes(b)] = sig + a * (1.0 - sig)
        return carry

    lax.fori_loop(0, rows // TILE, norm, 0)

    third = chan // 3
    span = plane * 16
    half = ny // 2
    stretches = ((0, nz // 2 + 1), (nz // 2 + 1, nz))
    upper, lower = pl.ds(0, half), pl.ds(half, half)

    def far(k):
        away = nz // 2 - lax.div(k + 1, 2)
        return lax.rem(z + (2 * lax.rem(k, 2) - 1) * away + nz, nz)

    def ring(step, leads, src_z, direction):
        buf, base = (rzr, at["zr"]) if direction > 0 else (rzl, at["zl"])
        part = upper if leads == (direction > 0) else lower
        slot = base + 2 * step + (0 if leads else 1)
        return remote(pz.at[src_z, part], buf.at[step, part], slot, along("z", nz, z, direction))

    def project(stretch):
        def step(k, carry):
            zz = far(k)
            cols = pl.ds(pl.multiple_of(zz * span, span), span)
            block = lax.dot_general(og_v[:, cols], act_v[...], (((0,), (0,)), ((), ())), preferred_element_type=F32)
            block = block.astype(BF16)
            for yy in range(ny):
                for xx in range(nx):
                    part = slice((yy * nx + xx) * 16, (yy * nx + xx) * 16 + 16)
                    px[xx, zz, yy] = block[part, 0:third]
                    py[yy, zz, xx] = block[part, third:2 * third]
                    pz[zz, yy, xx] = block[part, 2 * third:]
            for o in range(1, nx):
                peer = along("x", nx, x, o)
                slot = at["x1"] + stretch * (nx - 1) + o - 1
                remote(px.at[peer["x"], zz], rx.at[o - 1, zz], slot, peer).start()
            for o in range(1, ny):
                peer = along("y", ny, y, o)
                slot = at["y1"] + stretch * (ny - 1) + o - 1
                remote(py.at[peer["y"], zz], ry.at[o - 1, zz], slot, peer).start()
            if stretch == 0:
                @pl.when(k == 0)
                def _():
                    ring(0, True, zz, 1).start()
                    ring(0, True, zz, -1).start()

                @pl.when(k == 1)
                def _():
                    ring(1, False, zz, 1).start()

                @pl.when(k == 2)
                def _():
                    ring(1, False, zz, -1).start()

            return carry

        lax.fori_loop(*stretches[stretch], step, 0)

    def z_step(step, leads):
        for direction in (1, -1):
            dest = lax.rem(z + direction * (nz // 2 - step) + nz, nz)
            ring(step - 1, leads, dest, direction).wait_recv()
            buf = rzr if direction > 0 else rzl
            for yy in (range(half) if leads == (direction > 0) else range(half, ny)):
                pz[dest, yy] = (pz[dest, yy].astype(F32) + buf[step - 1, yy].astype(F32)).astype(BF16)
            ring(step, leads, dest, direction).start()

    loads["og"].wait()
    project(0)

    loads["w"].wait()

    def back(i, carry):
        r = pl.ds(pl.multiple_of(i * 128, 128), 128)
        ag_v[r, :] = jnp.dot(og_v[r, :], w_v[...], preferred_element_type=F32)
        return carry

    lax.fori_loop(0, rows // 128, back, 0)
    z_step(1, True)

    def grads(i, carry):
        r = pl.ds(pl.multiple_of(i * TILE, TILE), TILE)
        carry = list(carry)
        row_sum = jnp.zeros((TILE, LANE), F32)
        row_dot = jnp.zeros((TILE, LANE), F32)
        for b in range(blocks):
            g = ag_v[r, lanes(b)] * ds_v[r, lanes(b)]
            n = nm_v[r, lanes(b)]
            gn = g * n
            carry[b] = carry[b] + jnp.sum(gn.reshape(TILE // 8, 8, LANE), axis=0)
            carry[blocks + b] = carry[blocks + b] + jnp.sum(g.reshape(TILE // 8, 8, LANE), axis=0)
            gain = gain_v[lanes(b)].reshape(1, LANE)
            s = g * gain
            ag_v[r, lanes(b)] = s
            row_sum = row_sum + s
            row_dot = row_dot + gn * gain
        s2_s[0, r, :] = row_sum
        s2_s[1, r, :] = row_dot
        return tuple(carry)

    partial = lax.fori_loop(0, rows // TILE, grads, tuple(jnp.zeros((8, LANE), F32) for _ in range(2 * blocks)))

    def channel_sums(i, carry):
        for u in range(wide // 64):
            r = pl.ds(pl.multiple_of(i * wide + u * 64, 64), 64)
            for w in range(2):
                v = jnp.sum(s2_s[w, r, :], axis=1, keepdims=True)
                s2_s[w, r, :] = jnp.broadcast_to(v, (64, LANE))
        return carry

    lax.fori_loop(0, 2, channel_sums, 0)
    sums_copy = remote(s2_s, s2_r, at["sums"], other)
    sums_copy.start()

    project(1)
    z_step(2, False)

    gated_copy.wait_recv()
    for b in range(blocks):
        head = gh_r[:, lanes(b)].astype(F32)
        gt_v[b, 0:HALO, :] = jnp.where(line == 0, 0.0, head)

    sums_copy.wait_recv()

    def height(i, carry):
        r = pl.ds(pl.multiple_of(i * TILE, TILE), TILE)
        sums = (s2_s[0, r, :] + s2_r[0, r, :]) * (1.0 / total)
        dots = (s2_s[1, r, :] + s2_r[1, r, :]) * (1.0 / total)
        inv = iv_v[r, :]
        for b in range(blocks):
            hg_v[b, r, :] = inv * (ag_v[r, lanes(b)] - sums - nm_v[r, lanes(b)] * dots)
        return carry

    lax.fori_loop(0, rows // TILE, height, 0)
    for b in range(blocks):
        hh_s[:, lanes(b)] = hg_v[b, 0:HALO, :].astype(BF16)
    height_copy = remote(hh_s, hh_r, at["height"], before)
    height_copy.start()

    z_step(2, True)

    def gather(stretch, wide, me, got, out, got2, name, axis, size, own_size, own_me):
        lo, hi = stretches[stretch]
        for o in range(1, own_size):
            slot = at[name + "1"] + stretch * (own_size - 1) + o - 1
            part = got.at[o - 1, pl.ds(0, hi - lo)]
            remote(part, part, slot, other).wait_recv()

        def step(k, carry):
            zz = far(k)
            v = wide[me, zz].astype(F32)
            for o in range(own_size - 1):
                v = v + got[o, zz].astype(F32)
            v = v.astype(BF16)
            for w in range(size):
                out[w, zz] = v[w]
            for o in range(1, size):
                peer = along(axis, size, own_me, o)
                slot = at[name + "2"] + stretch * (size - 1) + o - 1
                remote(out.at[peer[axis], zz], got2.at[o - 1, zz], slot, peer).start()
            return carry

        lax.fori_loop(lo, hi, step, 0)

    def gather_both(stretch):
        gather(stretch, px, x, rx, sx, rx2, "x", "y", ny, nx, y)
        gather(stretch, py, y, ry, sy, ry2, "y", "x", nx, ny, x)

    small_rows = (taps + 2 + 7) // 8
    flat = sa.shape[0] * sa.shape[1]

    def tap_block(b):
        def step(t, acc):
            base = t * (8 * GROUP)
            h = [hg_v[b, pl.ds(pl.multiple_of(base + 8 * u, 8), 8), :] for u in range(GROUP)]
            acc = list(acc)
            for k in range(taps + 8 * (GROUP - 1)):
                v = gt_v[b, pl.ds(base + (HALO - reach) + k, 8), :]
                for u in range(GROUP):
                    if 0 <= k - 8 * u < taps:
                        acc[k - 8 * u] = acc[k - 8 * u] + h[u] * v
            return tuple(acc)

        acc = lax.fori_loop(
            0, rows // (8 * GROUP), step, tuple(jnp.zeros((8, LANE), F32) for _ in range(taps)))
        acc = list(acc) + [partial[b], partial[blocks + b]]
        lines = [jnp.sum(a, axis=0, keepdims=True) for a in acc]
        lines += [jnp.zeros((1, LANE), F32)] * (small_rows * 8 - len(lines))
        for t in range(small_rows):
            tile = b * small_rows + t
            sa[tile // 2, tile % 2] = jnp.concatenate(lines[t * 8:t * 8 + 8], axis=0)

    for b in range(blocks):
        tap_block(b)
        if b == 1:
            z_step(3, False)
        if b == 2:
            gather_both(0)
        if b == 3:
            z_step(3, True)
    for tile in range(blocks * small_rows, flat):
        sa[tile // 2, tile % 2] = jnp.zeros((8, LANE), F32)
    for o in range(1, plane):
        remote(sa.at[lax.rem(place + o, plane)], ra.at[o - 1], at["a1"] + o - 1, in_plane(o)).start()

    def z_done():
        for direction in (1, -1):
            for leads in (False, True):
                ring(nz // 2 - 1, leads, z, direction).wait_recv()
        for yy in range(ny):
            v = pz[z, yy].astype(F32) + rzr[nz // 2 - 1, yy].astype(F32) + rzl[nz // 2 - 1, yy].astype(F32)
            v = v.astype(BF16)
            for xx in range(nx):
                sz[xx, yy] = v[xx]
        for o in range(1, nx):
            peer = along("x", nx, x, o)
            remote(sz.at[peer["x"]], rz2.at[o - 1], at["z2"] + o - 1, peer).start()

    def small_plane():
        for o in range(1, plane):
            remote(sa.at[0], ra.at[o - 1], at["a1"] + o - 1, in_plane(o)).wait_recv()
        v = sa[place]
        for o in range(plane - 1):
            v = v + ra[o]
        fa[...] = v
        rza[z] = v
        for o in range(1, nz):
            remote(fa, rza.at[z], at["a2"] + z, along("z", nz, z, o)).start()

    def xy_third(stretch, own, me, got, out, last, name, size):
        lo, hi = stretches[stretch]
        for o in range(1, size):
            slot = at[name + "2"] + stretch * (size - 1) + o - 1
            part = got.at[o - 1, pl.ds(0, hi - lo)]
            remote(part, part, slot, other).wait_recv()

        def step(k, carry):
            zz = far(k)
            v = own[me, zz].astype(F32)
            for o in range(size - 1):
                v = v + got[o, zz].astype(F32)
            out[zz] = v.astype(BF16)

            @pl.when(k < nz - 1)
            def _():
                o = lax.rem(zz - z + nz, nz)
                remote(out.at[zz], last.at[o - 1], at[name + "3"] + o - 1, {"z": zz}).start()

            return carry

        lax.fori_loop(lo, hi, step, 0)

    def third_both(stretch):
        xy_third(stretch, sx, y, rx2, tx, rx3, "x", ny)
        xy_third(stretch, sy, x, ry2, ty, ry3, "y", nx)

    def z_third():
        for o in range(1, nx):
            remote(sz.at[0], rz2.at[o - 1], at["z2"] + o - 1, other).wait_recv()
        v = sz[x].astype(F32)
        for o in range(nx - 1):
            v = v + rz2[o].astype(F32)
        tz[...] = v.astype(BF16)
        for o in range(1, ny):
            peer = along("y", ny, y, o)
            remote(tz.at[peer["y"]], rz3.at[o - 1], at["z3"] + o - 1, peer).start()

    def small_line():
        for o in range(1, nz):
            zz = lax.rem(z + o, nz)
            remote(fa, rza.at[zz], at["a2"] + zz, other).wait_recv()
        v = rza[0]
        for zz in range(1, nz):
            v = v + rza[zz]
        fin[...] = v
        ag_a[place] = v
        for o in range(1, plane):
            remote(fin, ag_a.at[place], at["a3"] + o - 1, in_plane(o)).start()

    height_copy.wait_recv()
    for b in range(blocks):
        tail = hh_r[:, lanes(b)].astype(F32)
        hg_v[b, rows:rows + HALO, :] = jnp.where(line == count - 1, 0.0, tail)

    loads["taps"].wait()

    def gated_block(b):
        lines = taps_v[:, lanes(b)].astype(F32)
        spread = [jnp.broadcast_to(lines[j:j + 1, :], (8, LANE)) for j in range(taps)]

        def step(t, carry):
            base = t * (8 * GROUP)
            acc = [[None, None] for _ in range(GROUP)]
            for k in range(taps + 8 * (GROUP - 1)):
                v = hg_v[b, pl.ds(base + k, 8), :]
                for u in range(GROUP):
                    j = reach + 8 * u - k
                    if 0 <= j < taps:
                        term = spread[j] * v
                        old = acc[u][k % 2]
                        acc[u][k % 2] = term if old is None else old + term
            for u in range(0, GROUP, 2):
                r = pl.ds(pl.multiple_of(base + 8 * u, 16), 16)
                g = jnp.concatenate([acc[w][0] + acc[w][1] for w in (u, u + 1)], axis=0)
                s = sg_v[r, lanes(b)]
                gs = g * s
                gv_v[r, lanes(b)] = gs.astype(BF16)
                gg_v[r, lanes(b)] = (gs * cv_v[r, lanes(b)].astype(F32) * (1.0 - s)).astype(BF16)
            return carry

        lax.fori_loop(0, rows // (8 * GROUP), step, 0)

    for b in range(blocks):
        gated_block(b)
        if b == 0:
            gather_both(1)
        if b == 1:
            z_done()
            third_both(0)
        if b == 2:
            small_plane()
        if b == 3:
            third_both(1)
            z_third()
        if b == 5:
            small_line()

    for buf, own, last, name in ((0, tx, rx3, "x3"), (1, ty, ry3, "y3")):
        for o in range(1, nz):
            remote(own.at[0], last.at[o - 1], at[name] + o - 1, other).wait_recv()
        v = own[z].astype(F32)
        for o in range(nz - 1):
            v = v + last[o].astype(F32)
        proj_v[:, buf * third:(buf + 1) * third] = v
    for o in range(1, ny):
        remote(tz.at[0], rz3.at[o - 1], at["z3"] + o - 1, other).wait_recv()
    v = tz[y].astype(F32)
    for o in range(ny - 1):
        v = v + rz3[o].astype(F32)
    proj_v[:, 2 * third:] = v

    for o in range(1, plane):
        p = lax.rem(place - o + plane, plane)
        remote(fin, ag_a.at[p], at["a3"] + o - 1, other).wait_recv()
    for b in range(blocks):
        for t in range(small_rows):
            tile = b * small_rows + t
            v = ag_a[tile // 2, tile % 2]
            keep = min(8, taps - t * 8)
            if keep > 0:
                taps_o[t * 8:t * 8 + keep, lanes(b)] = v[0:keep]
            for row, out in ((taps, gain_o), (taps + 1, shift_o)):
                if row // 8 == t:
                    out[lanes(b)] = v[row % 8:row % 8 + 1].reshape(LANE)

    stat_copy.wait_send()
    gated_copy.wait_send()
    sums_copy.wait_send()
    height_copy.wait_send()
    for stretch, (lo, hi) in enumerate(stretches):
        some = pl.ds(0, hi - lo)
        for o in range(nx - 1):
            remote(px.at[0, some], rx.at[o, some], at["x1"] + stretch * (nx - 1) + o, other).wait_send()
            remote(sy.at[0, some], ry2.at[o, some], at["y2"] + stretch * (nx - 1) + o, other).wait_send()
        for o in range(ny - 1):
            remote(py.at[0, some], ry.at[o, some], at["y1"] + stretch * (ny - 1) + o, other).wait_send()
            remote(sx.at[0, some], rx2.at[o, some], at["x2"] + stretch * (ny - 1) + o, other).wait_send()
    for o in range(nx - 1):
        remote(sz.at[0], rz2.at[o], at["z2"] + o, other).wait_send()
    for o in range(ny - 1):
        remote(tz.at[0], rz3.at[o], at["z3"] + o, other).wait_send()
    for o in range(nz - 1):
        remote(tx.at[0], rx3.at[o], at["x3"] + o, other).wait_send()
        remote(ty.at[0], ry3.at[o], at["y3"] + o, other).wait_send()
    for step in range(nz // 2):
        for direction in (1, -1):
            ring(step, True, z, direction).wait_send()
            if step > 0:
                ring(step, False, z, direction).wait_send()
    for o in range(plane - 1):
        remote(sa.at[0], ra.at[o], at["a1"] + o, other).wait_send()
        remote(fin, ag_a.at[0], at["a3"] + o, other).wait_send()
    for o in range(1, nz):
        remote(fa, rza.at[z], at["a2"] + z, other).wait_send()


def local(conv_value, conv_gate, conv_out, conv_taps, norm_gain, norm_shift, proj_weight, out_grad):
    nz, ny, nx = (lax.axis_size(a) for a in SP)
    rows, chan = conv_value.shape
    depth = out_grad.shape[1]
    taps = conv_taps.shape[0]
    blocks = chan // LANE
    third = chan // 3
    plane = ny * nx
    slots, _ = layout(nz, ny, nx)
    vm = pltpu.VMEM
    small_rows = (taps + 2 + 7) // 8 * 8
    per = -(-blocks * small_rows // 8 // plane)
    scratch = [
        vm((rows, chan), BF16), vm((rows, depth), BF16), vm((depth, chan), BF16), vm((rows, chan), BF16),
        vm((rows, chan), BF16), vm((taps, chan), BF16), vm((chan,), F32), vm((chan,), F32),
        vm((2, rows, LANE), F32), vm((2, rows, LANE), F32), vm((2, rows, LANE), F32), vm((2, rows, LANE), F32),
        vm((rows, LANE), F32), vm((rows, chan), F32), vm((blocks, rows + HALO, LANE), F32), vm((rows, chan), F32),
        vm((rows, chan), F32), vm((rows, chan), BF16), vm((rows, chan), F32), vm((blocks, rows + HALO, LANE), F32),
        vm((HALO, chan), BF16), vm((HALO, chan), BF16), vm((HALO, chan), BF16), vm((HALO, chan), BF16),
        vm((nx, nz, ny, 16, third), BF16), vm((ny, nz, nx, 16, third), BF16), vm((nz, ny, nx, 16, third), BF16),
        vm((nx - 1, nz, ny, 16, third), BF16), vm((ny - 1, nz, nx, 16, third), BF16),
        vm((nz // 2, ny, nx, 16, third), BF16), vm((nz // 2, ny, nx, 16, third), BF16),
        vm((ny, nz, 16, third), BF16), vm((nx, nz, 16, third), BF16),
        vm((ny - 1, nz, 16, third), BF16), vm((nx - 1, nz, 16, third), BF16),
        vm((nz, 16, third), BF16), vm((nz, 16, third), BF16),
        vm((nz - 1, 16, third), BF16), vm((nz - 1, 16, third), BF16),
        vm((nx, ny, 16, third), BF16), vm((nx - 1, ny, 16, third), BF16),
        vm((ny, 16, third), BF16), vm((ny - 1, 16, third), BF16),
        vm((plane, per, 8, LANE), F32), vm((plane - 1, per, 8, LANE), F32), vm((per, 8, LANE), F32),
        vm((nz, per, 8, LANE), F32), vm((per, 8, LANE), F32), vm((plane, per, 8, LANE), F32),
        pltpu.SemaphoreType.DMA((8,)),
        pltpu.SemaphoreType.DMA((slots.used,)), pltpu.SemaphoreType.DMA((slots.used,)),
    ]
    anywhere = pl.BlockSpec(memory_space=pl.ANY)
    shapes = (
        ((rows, chan), BF16), ((rows, chan), BF16), ((taps, chan), F32), ((chan,), F32), ((chan,), F32), ((16, chan), F32),
    )
    held = pl.BlockSpec(memory_space=pltpu.VMEM)
    results = pl.pallas_call(
        functools.partial(kernel, (nz, ny, nx, rows, chan, depth, taps)),
        out_shape=tuple(pltpu.VMEM(*s) for s in shapes),
        in_specs=[anywhere] * 8,
        out_specs=(held,) * 6,
        scratch_shapes=scratch,
        compiler_params=pltpu.CompilerParams(
            collective_id=0, has_side_effects=True, vmem_limit_bytes=36 * 1024 * 1024),
        name="module_backward",
    )(*(pltpu.with_memory_space_constraint(a, pltpu.HBM) for a in (
        conv_value, conv_gate, conv_out, conv_taps, norm_gain, norm_shift, proj_weight, out_grad)))
    return pl.pallas_call(
        write_out,
        out_shape=tuple(jax.ShapeDtypeStruct(*s) for s in shapes),
        in_specs=[held] * 6,
        out_specs=(anywhere,) * 6,
        scratch_shapes=[pltpu.SemaphoreType.DMA((6,))],
        name="write_out",
    )(*(pltpu.with_memory_space_constraint(a, pltpu.VMEM) for a in results))


def write_out(*refs):
    sem = refs[12]
    copies = [pltpu.make_async_copy(refs[i], refs[6 + i], sem.at[i]) for i in range(6)]
    for c in copies:
        c.start()
    for c in copies:
        c.wait()


def solution(mesh):
    split = Mesh(mesh.devices.reshape(8, 4, 4, mesh.shape["tp"]), (*SP, "tp"))
    placed = (
        P(SP, "tp"), P(SP, "tp"), P(SP, "tp"), P(None, "tp"), P("tp"), P("tp"), P(None, "tp"), P(SP, None),
    )
    return jax.shard_map(
        local,
        mesh=split,
        in_specs=placed,
        out_specs=(P(SP, "tp"), P(SP, "tp"), P(None, "tp"), P("tp"), P("tp"), P(SP, "tp")),
        check_vma=False,
    )
```

time: 64 us -> 45.7 us (0.71)
  local copies, waits for them, and re-layouts: 10.2 us -> 0 us
  Pallas kernels: 52.8 us -> 44.9 us
    pallas_call x1, Pallas kernels: 52.8 us -> 43.6 us  [local(): pl.pallas_call(functools.partial(kernel, (nz, ny, nx, rows, chan, depth,...]
    unnamed x5 -> x0, local copies, waits for them, and re-layouts: 4.75 us -> none
    slice x2 -> x0, local copies, waits for them, and re-layouts: 2.92 us -> none  [the longest x1 1.54 us: local(): small[:taps]]
    reshape x2 -> x0, local copies, waits for them, and re-layouts: 2.53 us -> none  [the longest x1 1.27 us: local(): norm_gain.reshape(1, chan)]
    pallas_call x0 -> x1, Pallas kernels: none -> 1.23 us  [local(): pl.pallas_call(write_out, out_shape=tuple((jax.ShapeDtypeStruct(*s) for s...]
where the time goes in v2:
time: 45.7 us; the launch traced here: 45.5 us
  Pallas kernels  44.9 us (98%)
  between operations  0.64 us (1%)
    pallas_call x1, Pallas kernels, local(): pl.pallas_call(functools.partial(kernel, (nz, ny, nx, rows, chan, depth,...  43.6 us
    pallas_call x1, Pallas kernels, local(): pl.pallas_call(write_out, out_shape=tuple((jax.ShapeDtypeStruct(*s) for s...  1.23 us

profile of v2, /device:TPU:2, one launch (start us, length us, event | category | flops | bytes accessed | tf_op | source)
XLA Modules:
  0.0 45.5 jit_solution(11963621050297269041)
XLA Ops:
  0.6 43.6 %module_backward.1 = (bf16[512,768]{1,0:T(8,128)(2,1)S(1)}, bf16[512,768]{1,0:T(8,128)(2,1)S(1)}, f32[31,768]{1,0:T(8,128)S(1)}, f32[768]{0:T(1024)S(1)}, f32[768]{0:T(1024)S(1)}, /*index=5*/f32[16,768]{1,0:T(8,128)S(1)}) custom-call(bf16[512,768]{1,0:T(8,128)(2,1)} %refs_0_.1, bf16[512,768]{1,0:T(8,128)(2,1)} %refs_1_.1, bf16[512,768]{1,0:T(8,128)(2,1)} %refs_2_.1, ...), custom_call_target="tpu_custom_call" | custom-call | tf_op jit(solution)/shard_map/module_backward/pallas_call | solution.py:599
  44.3 1.2 %write_out.1 = (bf16[512,768]{1,0:T(8,128)(2,1)}, bf16[512,768]{1,0:T(8,128)(2,1)}, f32[31,768]{1,0:T(8,128)}, f32[768]{0:T(1024)}, f32[768]{0:T(1024)}, /*index=5*/f32[16,768]{1,0:T(8,128)}) custom-call(bf16[512,768]{1,0:T(8,128)(2,1)S(1)} %get-tuple-element.12.refs_0_, bf16[512,768]{1,0:T(8,128)(2,1)S(1)} %get-tuple-element.13.refs_1_, ...), custom_call_target="tpu_custom_call" | custom-call | tf_op jit(solution)/shard_map/write_out/pallas_call | solution.py:610

commit v3 on v2

v3 whole, which is shorter than its diff:
```python
import functools

import jax
import jax.numpy as jnp
from jax import lax
from jax.experimental import pallas as pl
from jax.experimental.pallas import tpu as pltpu
from jax.sharding import Mesh
from jax.sharding import PartitionSpec as P

MESH = pl.DeviceIdType.MESH
F32 = jnp.float32
BF16 = jnp.bfloat16
SP = ("z", "y", "x")
EPS = 1e-05
HALO = 32
LANE = 128
TILE = 32
GROUP = 8
FIRST = 128
FAR, NEAR, SUM = range(3)


class Slots:
    def __init__(self):
        self.used = 0

    def take(self, count):
        first = self.used
        self.used += count
        return first


def layout(nz, ny, nx):
    slots = Slots()
    plane = ny * nx
    return slots, {
        "stat": slots.take(1),
        "sums": slots.take(1),
        "gated": slots.take(1),
        "height": slots.take(1),
        "far": slots.take(2),
        "near": slots.take(2),
        "second": slots.take(2),
        "last": slots.take(1),
        "leads": slots.take(nz // 2),
        "trails": slots.take(nz // 2),
        "z2": slots.take(1),
        "z3": slots.take(1),
        "a1": slots.take(1),
        "a2": slots.take(1),
        "a3": slots.take(1),
    }


def kernel(sizes, *refs):
    nz, ny, nx, rows, chan, depth, taps = sizes
    cv_h, cg_h, co_h, taps_h, gain_h, shift_h, w_h, og_h, gv_v, gg_v, taps_o, gain_o, shift_o, proj_v = refs[:14]
    (co_v, og_v, ogt_v, w_v, cv_v, cg_v, taps_v, gain_v, shift_v, st_s, st_r, s2_s, s2_r, iv_v, sg_v, gt_v, nm_v, ds_v,
     act_v, ag_v, hg_v, gh_s, gh_r, hh_s, hh_r, pxy, pz, fxy, rxy, rzr, rzl, sxy, rxy2, txy, rxy3,
     sz, rz2, tz, rz3, stage, sa, ra, fa, rza, fin, ag_a, in_sem, ssem, rsem) = refs[14:]
    blocks = chan // LANE
    total = 2 * chan
    reach = taps - 1
    plane = ny * nx
    per = stage.shape[0] // plane
    px, fx, rx, sx, rx2, tx, rx3 = (a.at[0] for a in (pxy, fxy, rxy, sxy, rxy2, txy, rxy3))
    py, fy, ry, sy, ry2, ty, ry3 = (a.at[1] for a in (pxy, fxy, rxy, sxy, rxy2, txy, rxy3))
    _, at = layout(nz, ny, nx)
    z, y, x, core = (lax.axis_index(a) for a in ("z", "y", "x", "tp"))
    place = y * nx + x
    line = z * plane + place
    count = nz * plane

    def where(index):
        return {"z": lax.div(index, plane), "y": lax.rem(lax.div(index, nx), ny), "x": lax.rem(index, nx)}

    after = where(lax.rem(line + 1, count))
    before = where(lax.rem(line + count - 1, count))
    other = {"tp": 1 - core}

    def along(axis, size, me, step):
        return {axis: lax.rem(me + step + size, size)}

    def in_plane(step):
        p = lax.rem(place + step, plane)
        return {"y": lax.div(p, nx), "x": lax.rem(p, nx)}

    def remote(src, dst, slot, target):
        return pltpu.make_async_remote_copy(
            src_ref=src, dst_ref=dst, send_sem=ssem.at[slot], recv_sem=rsem.at[slot],
            device_id=target, device_id_type=MESH)

    loads = {}
    for slot, (name, src, dst) in enumerate((
            ("co", co_h, co_v), ("gain", gain_h, gain_v), ("shift", shift_h, shift_v), ("cg", cg_h, cg_v),
            ("cv", cv_h, cv_v), ("og", og_h, og_v), ("w", w_h, w_v), ("taps", taps_h, taps_v))):
        loads[name] = pltpu.make_async_copy(src, dst, in_sem.at[slot])
        loads[name].start()

    barrier = pltpu.get_barrier_semaphore()
    peers = [other, after, before]
    peers += [in_plane(o) for o in range(1, plane)]
    peers += [along("z", nz, z, o) for o in range(1, nz)]
    for peer in peers:
        pl.semaphore_signal(barrier, inc=1, device_id=peer, device_id_type=MESH)

    def lanes(b):
        return slice(b * LANE, (b + 1) * LANE)

    loads["co"].wait()

    wide = rows // 2

    def means(i, carry):
        for u in range(wide // 64):
            r = pl.ds(pl.multiple_of(i * wide + u * 64, 64), 64)
            m = jnp.sum(co_v[r, :].astype(F32), axis=1, keepdims=True) * (1.0 / chan)
            st_s[0, r, :] = jnp.broadcast_to(m, (64, LANE))
        return carry

    lax.fori_loop(0, 2, means, 0)

    def spreads(i, carry):
        for u in range(wide // 64):
            r = pl.ds(pl.multiple_of(i * wide + u * 64, 64), 64)
            m = st_s[0, r, :]
            q = jnp.zeros((64, LANE), F32)
            for b in range(blocks):
                d = co_v[r, lanes(b)].astype(F32) - m
                q = q + d * d
            st_s[1, r, :] = jnp.broadcast_to(jnp.sum(q, axis=1, keepdims=True), (64, LANE))
        return carry

    lax.fori_loop(0, 2, spreads, 0)

    pl.semaphore_wait(barrier, len(peers))
    stat_copy = remote(st_s, st_r, at["stat"], other)
    stat_copy.start()
    loads["cg"].wait()
    loads["cv"].wait()

    def gates(i, carry):
        r = pl.ds(pl.multiple_of(i * TILE, TILE), TILE)
        up = pl.ds(pl.multiple_of(i * TILE + HALO, TILE), TILE)
        for b in range(blocks):
            s = 0.5 * jnp.tanh(0.5 * cg_v[r, lanes(b)].astype(F32)) + 0.5
            sg_v[r, lanes(b)] = s
            gt_v[b, up, :] = (cv_v[r, lanes(b)].astype(F32) * s).astype(BF16).astype(F32)
        return carry

    lax.fori_loop(0, rows // TILE, gates, 0)
    for b in range(blocks):
        gh_s[:, lanes(b)] = gt_v[b, rows:rows + HALO, :].astype(BF16)

    gated_copy = remote(gh_s, gh_r, at["gated"], after)

    @pl.when(line < count - 1)
    def _():
        gated_copy.start()


    loads["og"].wait()

    span = plane * 16

    def far(k):
        away = nz // 2 - lax.div(k + 1, 2)
        return lax.rem(z + (2 * lax.rem(k, 2) - 1) * away + nz, nz)

    def turn(k, carry):
        cols = pl.ds(pl.multiple_of(far(k) * span, span), span)
        ogt_v[pl.ds(pl.multiple_of(k * span, span), span), :] = og_v[:, cols].T
        return carry

    lax.fori_loop(0, nz, turn, 0)
    loads["w"].wait()
    ag_v[0:FIRST, :] = jnp.dot(og_v[0:FIRST, :], w_v[...], preferred_element_type=F32)
    loads["gain"].wait()
    loads["shift"].wait()
    stat_copy.wait_recv()

    def norm(i, carry):
        r = pl.ds(pl.multiple_of(i * TILE, TILE), TILE)
        m1, m2 = st_s[0, r, :], st_r[0, r, :]
        gap = m1 - m2
        mean = 0.5 * (m1 + m2)
        inv = lax.rsqrt((st_s[1, r, :] + st_r[1, r, :] + gap * gap * (chan / 2)) * (1.0 / total) + EPS)
        iv_v[r, :] = inv
        for b in range(blocks):
            n = (co_v[r, lanes(b)].astype(F32) - mean) * inv
            s = n * gain_v[lanes(b)].reshape(1, LANE) + shift_v[lanes(b)].reshape(1, LANE)
            sig = 0.5 * jnp.tanh(0.5 * s) + 0.5
            a = s * sig
            act_v[r, lanes(b)] = a.astype(BF16)
            nm_v[r, lanes(b)] = n
            ds_v[r, lanes(b)] = sig + a * (1.0 - sig)
        return carry

    lax.fori_loop(0, rows // TILE, norm, 0)

    third = chan // 3
    half = ny // 2
    stretches = ((0, nz // 2), (nz // 2, nz))
    upper, lower = pl.ds(0, half), pl.ds(half, half)

    def ring(step, leads, src_z, direction):
        buf = rzr if direction > 0 else rzl
        part = upper if leads == (direction > 0) else lower
        slot = at["leads" if leads else "trails"] + step
        return remote(pz.at[src_z, part], buf.at[step, part], slot, along("z", nz, z, direction))

    rings = {"x": (px, fx, rx, x), "y": (py, fy, ry, y)}

    def hop(axis, stretch, kind, direction, lines):
        wide, far_got, got, me = rings[axis]
        d = 0 if direction > 0 else 1
        mine, rest = (upper, lower) if direction > 0 else (lower, upper)
        slot = at["far" if kind == FAR else "near"] + stretch
        peer = along(axis, 4, me, direction)
        if kind == FAR:
            return remote(wide.at[lax.rem(me + 2, 4), lines, mine], far_got.at[d, lines], slot, peer)
        part = rest if kind == NEAR else mine
        return remote(wide.at[peer[axis], lines, part], got.at[d, lines, part], slot, peer)

    def relay(stretch):
        lo, hi = stretches[stretch]
        part = fxy.at[:, :, pl.ds(0, hi - lo)]
        remote(part, part, at["far"] + stretch, other).wait_recv()
        for axis in ("x", "y"):
            wide, far_got, _, me = rings[axis]
            for direction in (1, -1):
                d, first = (0, 0) if direction > 0 else (1, half)
                dest = lax.rem(me + direction + 4, 4)

                def step(k, carry):
                    for w in range(half):
                        v = wide[dest, k, first + w].astype(F32) + far_got[d, k, w].astype(F32)
                        wide[dest, k, first + w] = v.astype(BF16)
                    return carry

                lax.fori_loop(lo, hi, step, 0)
                hop(axis, stretch, SUM, direction, pl.ds(lo, hi - lo)).start()

    def ring_wait(step, leads):
        return remote(pz.at[0], pz.at[0], at["leads" if leads else "trails"] + step, other)

    def project(stretch):
        def step(i, carry):
            lines = pl.ds(pl.multiple_of(i * 2 * span, span), 2 * span)
            both = jnp.dot(ogt_v[lines, :], act_v[...], preferred_element_type=F32)
            for u in range(2):
                k = 2 * i + u
                zz = far(k)
                block = both[u * span:(u + 1) * span].astype(BF16)
                for yy in range(ny):
                    for xx in range(nx):
                        part = slice((yy * nx + xx) * 16, (yy * nx + xx) * 16 + 16)
                        px[xx, k, yy] = block[part, 0:third]
                        py[yy, k, xx] = block[part, third:2 * third]
                        pz[zz, yy, xx] = block[part, 2 * third:]
            if stretch == 0:
                @pl.when(i == 0)
                def _():
                    for direction in (1, -1):
                        ring(0, True, far(0), direction).start()
                    ring(1, False, far(1), 1).start()

                @pl.when(i == 1)
                def _():
                    ring(1, False, far(2), -1).start()

            return carry

        lo, hi = stretches[stretch]
        lax.fori_loop(lo // 2, hi // 2, step, 0)
        for kind in (FAR, NEAR):
            for axis in ("x", "y"):
                for direction in (1, -1):
                    hop(axis, stretch, kind, direction, pl.ds(lo, hi - lo)).start()

    def z_step(step, leads):
        ring_wait(step - 1, leads).wait_recv()
        for direction in (1, -1):
            dest = lax.rem(z + direction * (nz // 2 - step) + nz, nz)
            buf = rzr if direction > 0 else rzl
            for yy in (range(half) if leads == (direction > 0) else range(half, ny)):
                pz[dest, yy] = (pz[dest, yy].astype(F32) + buf[step - 1, yy].astype(F32)).astype(BF16)
            ring(step, leads, dest, direction).start()

    project(0)

    ag_v[FIRST:, :] = jnp.dot(og_v[FIRST:, :], w_v[...], preferred_element_type=F32)

    def grads(i, carry):
        r = pl.ds(pl.multiple_of(i * TILE, TILE), TILE)
        carry = list(carry)
        row_sum = jnp.zeros((TILE, LANE), F32)
        row_dot = jnp.zeros((TILE, LANE), F32)
        for b in range(blocks):
            g = ag_v[r, lanes(b)] * ds_v[r, lanes(b)]
            n = nm_v[r, lanes(b)]
            gn = g * n
            carry[b] = carry[b] + jnp.sum(gn.reshape(TILE // 8, 8, LANE), axis=0)
            carry[blocks + b] = carry[blocks + b] + jnp.sum(g.reshape(TILE // 8, 8, LANE), axis=0)
            gain = gain_v[lanes(b)].reshape(1, LANE)
            s = g * gain
            ag_v[r, lanes(b)] = s
            row_sum = row_sum + s
            row_dot = row_dot + gn * gain
        s2_s[0, r, :] = row_sum
        s2_s[1, r, :] = row_dot
        return tuple(carry)

    partial = lax.fori_loop(0, rows // TILE, grads, tuple(jnp.zeros((8, LANE), F32) for _ in range(2 * blocks)))

    def channel_sums(i, carry):
        for u in range(wide // 64):
            r = pl.ds(pl.multiple_of(i * wide + u * 64, 64), 64)
            for w in range(2):
                v = jnp.sum(s2_s[w, r, :], axis=1, keepdims=True)
                s2_s[w, r, :] = jnp.broadcast_to(v, (64, LANE))
        return carry

    lax.fori_loop(0, 2, channel_sums, 0)
    sums_copy = remote(s2_s, s2_r, at["sums"], other)
    sums_copy.start()

    project(1)
    relay(0)
    z_step(1, True)

    @pl.when(line > 0)
    def _():
        gated_copy.wait_recv()

    for b in range(blocks):
        head = gh_r[:, lanes(b)].astype(F32)
        gt_v[b, 0:HALO, :] = jnp.where(line == 0, 0.0, head)

    sums_copy.wait_recv()

    def height(i, carry):
        r = pl.ds(pl.multiple_of(i * TILE, TILE), TILE)
        sums = (s2_s[0, r, :] + s2_r[0, r, :]) * (1.0 / total)
        dots = (s2_s[1, r, :] + s2_r[1, r, :]) * (1.0 / total)
        inv = iv_v[r, :]
        for b in range(blocks):
            hg_v[b, r, :] = inv * (ag_v[r, lanes(b)] - sums - nm_v[r, lanes(b)] * dots)
        return carry

    lax.fori_loop(0, rows // TILE, height, 0)
    for b in range(blocks):
        hh_s[:, lanes(b)] = hg_v[b, 0:HALO, :].astype(BF16)
    height_copy = remote(hh_s, hh_r, at["height"], before)

    @pl.when(line > 0)
    def _():
        height_copy.start()


    def gather(stretch, wide, me, got, out, got2, axis, size, own_me):
        lo, hi = stretches[stretch]

        def step(k, carry):
            v = (wide[me, k].astype(F32) + got[0, k].astype(F32) + got[1, k].astype(F32)).astype(BF16)
            for w in range(size):
                out[w, k] = v[w]
            return carry

        lax.fori_loop(lo, hi, step, 0)
        some = pl.ds(lo, hi - lo)
        for o in range(1, size):
            peer = along(axis, size, own_me, o)
            remote(out.at[peer[axis], some], got2.at[o - 1, some], at["second"] + stretch, peer).start()

    def gather_both(stretch):
        lo, hi = stretches[stretch]
        part = rxy.at[:, :, pl.ds(0, hi - lo)]
        remote(part, part, at["near"] + stretch, other).wait_recv()
        gather(stretch, px, x, rx, sx, rx2, "y", ny, y)
        gather(stretch, py, y, ry, sy, ry2, "x", nx, x)

    used = blocks * (taps + 2)
    stage[used:, :] = jnp.zeros((stage.shape[0] - used, LANE), F32)

    def tap_block(b):
        def step(t, acc):
            base = t * (8 * GROUP)
            h = [hg_v[b, pl.ds(pl.multiple_of(base + 8 * u, 8), 8), :] for u in range(GROUP)]
            acc = list(acc)
            for k in range(taps + 8 * (GROUP - 1)):
                v = gt_v[b, pl.ds(base + (HALO - reach) + k, 8), :]
                for u in range(GROUP):
                    if 0 <= k - 8 * u < taps:
                        acc[k - 8 * u] = acc[k - 8 * u] + h[u] * v
            return tuple(acc)

        acc = lax.fori_loop(
            0, rows // (8 * GROUP), step, tuple(jnp.zeros((8, LANE), F32) for _ in range(taps)))
        acc = list(acc) + [partial[b], partial[blocks + b]]
        for j, a in enumerate(acc):
            row = b * (taps + 2) + j
            stage[row:row + 1, :] = jnp.sum(a, axis=0, keepdims=True)

    for b in range(blocks):
        tap_block(b)
        if b == 0:
            z_step(2, False)
        if b == 3:
            z_step(2, True)
            relay(1)
    for p in range(plane):
        sa[p] = stage[p * per:(p + 1) * per, :].astype(BF16)
    for o in range(1, plane):
        remote(sa.at[lax.rem(place + o, plane)], ra.at[o - 1], at["a1"], in_plane(o)).start()

    def z_done():
        for leads in (False, True):
            ring_wait(nz // 2 - 1, leads).wait_recv()
        for yy in range(ny):
            v = pz[z, yy].astype(F32) + rzr[nz // 2 - 1, yy].astype(F32) + rzl[nz // 2 - 1, yy].astype(F32)
            v = v.astype(BF16)
            for xx in range(nx):
                sz[xx, yy] = v[xx]
        for o in range(1, nx):
            peer = along("x", nx, x, o)
            remote(sz.at[peer["x"]], rz2.at[o - 1], at["z2"], peer).start()

    def small_plane():
        remote(ra, ra, at["a1"], other).wait_recv()
        v = stage[pl.ds(pl.multiple_of(place * per, 8), per), :]
        for o in range(plane - 1):
            v = v + ra[o].astype(F32)
        fa[...] = v
        rza[z] = v
        for o in range(1, nz):
            remote(fa, rza.at[z], at["a2"], along("z", nz, z, o)).start()

    def xy_third(stretch, own, me, got, out, last, size):
        lo, hi = stretches[stretch]
        def step(k, carry):
            zz = far(k)
            v = own[me, k].astype(F32)
            for o in range(size - 1):
                v = v + got[o, k].astype(F32)
            out[k] = v.astype(BF16)

            @pl.when(k < nz - 1)
            def _():
                o = lax.rem(zz - z + nz, nz)
                remote(out.at[k], last.at[o - 1], at["last"], {"z": zz}).start()

            return carry

        lax.fori_loop(lo, hi, step, 0)

    def third_both(stretch):
        lo, hi = stretches[stretch]
        part = rxy2.at[:, :, pl.ds(0, hi - lo)]
        remote(part, part, at["second"] + stretch, other).wait_recv()
        xy_third(stretch, sx, y, rx2, tx, rx3, ny)
        xy_third(stretch, sy, x, ry2, ty, ry3, nx)

    def z_third():
        remote(rz2, rz2, at["z2"], other).wait_recv()
        v = sz[x].astype(F32)
        for o in range(nx - 1):
            v = v + rz2[o].astype(F32)
        tz[...] = v.astype(BF16)
        for o in range(1, ny):
            peer = along("y", ny, y, o)
            remote(tz.at[peer["y"]], rz3.at[o - 1], at["z3"], peer).start()

    def small_line():
        rest = rza.at[pl.ds(0, nz - 1)]
        remote(rest, rest, at["a2"], other).wait_recv()
        v = rza[0]
        for zz in range(1, nz):
            v = v + rza[zz]
        fin[...] = v
        ag_a[place] = v
        for o in range(1, plane):
            remote(fin, ag_a.at[place], at["a3"], in_plane(o)).start()

    z_step(3, False)
    gather_both(0)

    @pl.when(line < count - 1)
    def _():
        height_copy.wait_recv()

    for b in range(blocks):
        tail = hh_r[:, lanes(b)].astype(F32)
        hg_v[b, rows:rows + HALO, :] = jnp.where(line == count - 1, 0.0, tail)

    loads["taps"].wait()

    def gated_block(b):
        lines = taps_v[:, lanes(b)].astype(F32)
        spread = [jnp.broadcast_to(lines[j:j + 1, :], (8, LANE)) for j in range(taps)]

        def step(t, carry):
            base = t * (8 * GROUP)
            acc = [None] * GROUP
            for k in range(taps + 8 * (GROUP - 1)):
                v = hg_v[b, pl.ds(base + k, 8), :]
                for u in range(GROUP):
                    j = reach + 8 * u - k
                    if 0 <= j < taps:
                        term = spread[j] * v
                        acc[u] = term if acc[u] is None else acc[u] + term
            for u in range(0, GROUP, 2):
                r = pl.ds(pl.multiple_of(base + 8 * u, 16), 16)
                g = jnp.concatenate(acc[u:u + 2], axis=0)
                s = sg_v[r, lanes(b)]
                gs = g * s
                gv_v[r, lanes(b)] = gs.astype(BF16)
                gg_v[r, lanes(b)] = (gs * cv_v[r, lanes(b)].astype(F32) * (1.0 - s)).astype(BF16)
            return carry

        lax.fori_loop(0, rows // (8 * GROUP), step, 0)

    for b in range(blocks):
        gated_block(b)
        if b == 1:
            z_step(3, True)
            gather_both(1)
        if b == 3:
            small_plane()
        if b == 4:
            third_both(0)
        if b == 5:
            third_both(1)
            z_done()
            small_line()
            z_third()

    remote(rxy3, rxy3, at["last"], other).wait_recv()
    for buf, own, last in ((0, tx, rx3), (1, ty, ry3)):
        v = own[nz - 1].astype(F32)
        for o in range(nz - 1):
            v = v + last[o].astype(F32)
        proj_v[:, buf * third:(buf + 1) * third] = v
    remote(rz3, rz3, at["z3"], other).wait_recv()
    v = tz[y].astype(F32)
    for o in range(ny - 1):
        v = v + rz3[o].astype(F32)
    proj_v[:, 2 * third:] = v

    rest = ag_a.at[pl.ds(0, plane - 1)]
    remote(rest, rest, at["a3"], other).wait_recv()
    for b in range(blocks):
        for j in range(taps + 2):
            row = b * (taps + 2) + j
            v = ag_a[row // per, row % per:row % per + 1, :]
            if j < taps:
                taps_o[j:j + 1, lanes(b)] = v
            else:
                (gain_o if j == taps else shift_o)[lanes(b)] = v.reshape(LANE)

    stat_copy.wait_send()

    @pl.when(line < count - 1)
    def _():
        gated_copy.wait_send()

    sums_copy.wait_send()

    @pl.when(line > 0)
    def _():
        height_copy.wait_send()

    for stretch, (lo, hi) in enumerate(stretches):
        some = pl.ds(0, hi - lo)
        for name, buf in (("far", fxy), ("near", rxy), ("second", rxy2)):
            part = buf.at[:, :, some]
            remote(part, part, at[name] + stretch, other).wait_send()
    for step in range(nz // 2):
        ring_wait(step, True).wait_send()
        if step > 0:
            ring_wait(step, False).wait_send()
    for name, part in (("last", rxy3), ("z2", rz2), ("z3", rz3), ("a1", ra), ("a2", rza.at[pl.ds(0, nz - 1)]), ("a3", rest)):
        remote(part, part, at[name], other).wait_send()


def local(conv_value, conv_gate, conv_out, conv_taps, norm_gain, norm_shift, proj_weight, out_grad):
    nz, ny, nx = (lax.axis_size(a) for a in SP)
    rows, chan = conv_value.shape
    depth = out_grad.shape[1]
    taps = conv_taps.shape[0]
    blocks = chan // LANE
    third = chan // 3
    plane = ny * nx
    slots, _ = layout(nz, ny, nx)
    vm = pltpu.VMEM
    per = -(-(blocks * (taps + 2)) // (16 * plane)) * 16
    scratch = [
        vm((rows, chan), BF16), vm((rows, depth), BF16), vm((depth, rows), BF16), vm((depth, chan), BF16), vm((rows, chan), BF16),
        vm((rows, chan), BF16), vm((taps, chan), BF16), vm((chan,), F32), vm((chan,), F32),
        vm((2, rows, LANE), F32), vm((2, rows, LANE), F32), vm((2, rows, LANE), F32), vm((2, rows, LANE), F32),
        vm((rows, LANE), F32), vm((rows, chan), F32), vm((blocks, rows + HALO, LANE), F32), vm((rows, chan), F32),
        vm((rows, chan), F32), vm((rows, chan), BF16), vm((rows, chan), F32), vm((blocks, rows + HALO, LANE), F32),
        vm((HALO, chan), BF16), vm((HALO, chan), BF16), vm((HALO, chan), BF16), vm((HALO, chan), BF16),
        vm((2, 4, nz, 4, 16, third), BF16), vm((nz, 4, 4, 16, third), BF16),
        vm((2, 2, nz, 2, 16, third), BF16), vm((2, 2, nz, 4, 16, third), BF16),
        vm((nz // 2, 4, 4, 16, third), BF16), vm((nz // 2, 4, 4, 16, third), BF16),
        vm((2, 4, nz, 16, third), BF16), vm((2, 3, nz, 16, third), BF16),
        vm((2, nz, 16, third), BF16), vm((2, nz - 1, 16, third), BF16),
        vm((nx, ny, 16, third), BF16), vm((nx - 1, ny, 16, third), BF16),
        vm((ny, 16, third), BF16), vm((ny - 1, 16, third), BF16),
        vm((plane * per, LANE), F32), vm((plane, per, LANE), BF16), vm((plane - 1, per, LANE), BF16), vm((per, LANE), F32),
        vm((nz, per, LANE), F32), vm((per, LANE), F32), vm((plane, per, LANE), F32),
        pltpu.SemaphoreType.DMA((8,)),
        pltpu.SemaphoreType.DMA((slots.used,)), pltpu.SemaphoreType.DMA((slots.used,)),
    ]
    anywhere = pl.BlockSpec(memory_space=pl.ANY)
    shapes = (
        ((rows, chan), BF16), ((rows, chan), BF16), ((taps, chan), F32), ((chan,), F32), ((chan,), F32), ((16, chan), F32),
    )
    held = pl.BlockSpec(memory_space=pltpu.VMEM)
    results = pl.pallas_call(
        functools.partial(kernel, (nz, ny, nx, rows, chan, depth, taps)),
        out_shape=tuple(pltpu.VMEM(*s) for s in shapes),
        in_specs=[anywhere] * 8,
        out_specs=(held,) * 6,
        scratch_shapes=scratch,
        compiler_params=pltpu.CompilerParams(
            collective_id=0, has_side_effects=True, vmem_limit_bytes=36 * 1024 * 1024),
        name="module_backward",
    )(*(pltpu.with_memory_space_constraint(a, pltpu.HBM) for a in (
        conv_value, conv_gate, conv_out, conv_taps, norm_gain, norm_shift, proj_weight, out_grad)))
    return pl.pallas_call(
        write_out,
        out_shape=tuple(jax.ShapeDtypeStruct(*s) for s in shapes),
        in_specs=[held] * 6,
        out_specs=(anywhere,) * 6,
        scratch_shapes=[pltpu.SemaphoreType.DMA((6,))],
        name="write_out",
    )(*(pltpu.with_memory_space_constraint(a, pltpu.VMEM) for a in results))


def write_out(*refs):
    sem = refs[12]
    copies = [pltpu.make_async_copy(refs[i], refs[6 + i], sem.at[i]) for i in range(6)]
    for c in copies:
        c.start()
    for c in copies:
        c.wait()


def solution(mesh):
    split = Mesh(mesh.devices.reshape(8, 4, 4, mesh.shape["tp"]), (*SP, "tp"))
    placed = (
        P(SP, "tp"), P(SP, "tp"), P(SP, "tp"), P(None, "tp"), P("tp"), P("tp"), P(None, "tp"), P(SP, None),
    )
    return jax.shard_map(
        local,
        mesh=split,
        in_specs=placed,
        out_specs=(P(SP, "tp"), P(SP, "tp"), P(None, "tp"), P("tp"), P("tp"), P(SP, "tp")),
        check_vma=False,
    )
```

time: 45.7 us -> 42.3 us (0.926)
  Pallas kernels: 44.9 us -> 41.5 us
    pallas_call x1, Pallas kernels: 43.6 us -> 40.3 us  [local(): pl.pallas_call(functools.partial(kernel, (nz, ny, nx, rows, chan, depth,...]
where the time goes in v3:
time: 42.3 us; the launch traced here: 42.2 us
  Pallas kernels  41.5 us (98%)
  between operations  0.64 us (2%)
    pallas_call x1, Pallas kernels, local(): pl.pallas_call(functools.partial(kernel, (nz, ny, nx, rows, chan, depth,...  40.3 us
    pallas_call x1, Pallas kernels, local(): pl.pallas_call(write_out, out_shape=tuple((jax.ShapeDtypeStruct(*s) for s...  1.23 us

profile of v3, /device:TPU:2, one launch (start us, length us, event | category | flops | bytes accessed | tf_op | source)
XLA Modules:
  0.0 42.2 jit_solution(9960321512148595925)
XLA Ops:
  0.6 40.3 %module_backward.1 = (bf16[512,768]{1,0:T(8,128)(2,1)S(1)}, bf16[512,768]{1,0:T(8,128)(2,1)S(1)}, f32[31,768]{1,0:T(8,128)S(1)}, f32[768]{0:T(1024)S(1)}, f32[768]{0:T(1024)S(1)}, /*index=5*/f32[16,768]{1,0:T(8,128)S(1)}) custom-call(bf16[512,768]{1,0:T(8,128)(2,1)} %refs_0_.1, bf16[512,768]{1,0:T(8,128)(2,1)} %refs_1_.1, bf16[512,768]{1,0:T(8,128)(2,1)} %refs_2_.1, ...), custom_call_target="tpu_custom_call" | custom-call | tf_op jit(solution)/shard_map/module_backward/pallas_call | solution.py:622
  41.0 1.2 %write_out.1 = (bf16[512,768]{1,0:T(8,128)(2,1)}, bf16[512,768]{1,0:T(8,128)(2,1)}, f32[31,768]{1,0:T(8,128)}, f32[768]{0:T(1024)}, f32[768]{0:T(1024)}, /*index=5*/f32[16,768]{1,0:T(8,128)}) custom-call(bf16[512,768]{1,0:T(8,128)(2,1)S(1)} %get-tuple-element.12.refs_0_, bf16[512,768]{1,0:T(8,128)(2,1)S(1)} %get-tuple-element.13.refs_1_, ...), custom_call_target="tpu_custom_call" | custom-call | tf_op jit(solution)/shard_map/write_out/pallas_call | solution.py:633

commit v4 on v3

--- a/solution.py
+++ b/solution.py
@@ -91,19 +91,23 @@
             src_ref=src, dst_ref=dst, send_sem=ssem.at[slot], recv_sem=rsem.at[slot],
             device_id=target, device_id_type=MESH)
 
+    first_load = pltpu.make_async_copy(co_h, co_v, in_sem.at[0])
+    first_load.start()
+
+    barrier = pltpu.get_barrier_semaphore()
+    peers = [along("z", nz, z, o) for o in sorted(range(1, nz), key=lambda o: -min(o, nz - o))]
+    peers += [in_plane(o) for o in range(plane - 1, 0, -1)]
+    peers += [after, before, other]
+    for peer in peers:
+        pl.semaphore_signal(barrier, inc=1, device_id=peer, device_id_type=MESH)
+
     loads = {}
     for slot, (name, src, dst) in enumerate((
             ("co", co_h, co_v), ("gain", gain_h, gain_v), ("shift", shift_h, shift_v), ("cg", cg_h, cg_v),
             ("cv", cv_h, cv_v), ("og", og_h, og_v), ("w", w_h, w_v), ("taps", taps_h, taps_v))):
         loads[name] = pltpu.make_async_copy(src, dst, in_sem.at[slot])
-        loads[name].start()
-
-    barrier = pltpu.get_barrier_semaphore()
-    peers = [other, after, before]
-    peers += [in_plane(o) for o in range(1, plane)]
-    peers += [along("z", nz, z, o) for o in range(1, nz)]
-    for peer in peers:
-        pl.semaphore_signal(barrier, inc=1, device_id=peer, device_id_type=MESH)
+        if slot > 0:
+            loads[name].start()
 
     def lanes(b):
         return slice(b * LANE, (b + 1) * LANE)
@@ -312,19 +316,20 @@
         s2_s[1, r, :] = row_dot
         return tuple(carry)
 
-    partial = lax.fori_loop(0, rows // TILE, grads, tuple(jnp.zeros((8, LANE), F32) for _ in range(2 * blocks)))
-
-    def channel_sums(i, carry):
+    def channel_sums(i):
         for u in range(wide // 64):
-            r = pl.ds(pl.multiple_of(i * wide + u * 64, 64), 64)
+            r = pl.ds(i * wide + u * 64, 64)
             for w in range(2):
                 v = jnp.sum(s2_s[w, r, :], axis=1, keepdims=True)
                 s2_s[w, r, :] = jnp.broadcast_to(v, (64, LANE))
-        return carry
-
-    lax.fori_loop(0, 2, channel_sums, 0)
+
+    partial = tuple(jnp.zeros((8, LANE), F32) for _ in range(2 * blocks))
+    for i in range(2):
+        partial = lax.fori_loop(i * wide // TILE, (i + 1) * wide // TILE, grads, partial)
+        channel_sums(i)
+        part = pl.ds(i * wide, wide)
+        remote(s2_s.at[:, part], s2_r.at[:, part], at["sums"], other).start()
     sums_copy = remote(s2_s, s2_r, at["sums"], other)
-    sums_copy.start()
 
     project(1)
     relay(0)
@@ -405,9 +410,9 @@
 
     for b in range(blocks):
         tap_block(b)
-        if b == 0:
+        if b == 1:
             z_step(2, False)
-        if b == 3:
+        if b == 4:
             z_step(2, True)
             relay(1)
     for p in range(plane):
@@ -432,8 +437,8 @@
         v = stage[pl.ds(pl.multiple_of(place * per, 8), per), :]
         for o in range(plane - 1):
             v = v + ra[o].astype(F32)
-        fa[...] = v
-        rza[z] = v
+        fa[...] = v.astype(BF16)
+        rza[z] = v.astype(BF16)
         for o in range(1, nz):
             remote(fa, rza.at[z], at["a2"], along("z", nz, z, o)).start()
 
@@ -475,11 +480,11 @@
     def small_line():
         rest = rza.at[pl.ds(0, nz - 1)]
         remote(rest, rest, at["a2"], other).wait_recv()
-        v = rza[0]
+        v = rza[0].astype(F32)
         for zz in range(1, nz):
-            v = v + rza[zz]
-        fin[...] = v
-        ag_a[place] = v
+            v = v + rza[zz].astype(F32)
+        fin[...] = v.astype(BF16)
+        ag_a[place] = v.astype(BF16)
         for o in range(1, plane):
             remote(fin, ag_a.at[place], at["a3"], in_plane(o)).start()
 
@@ -526,13 +531,14 @@
         if b == 1:
             z_step(3, True)
             gather_both(1)
+        if b == 2:
+            small_plane()
         if b == 3:
-            small_plane()
+            z_done()
+            third_both(0)
         if b == 4:
-            third_both(0)
+            third_both(1)
         if b == 5:
-            third_both(1)
-            z_done()
             small_line()
             z_third()
 
@@ -550,10 +556,12 @@
 
     rest = ag_a.at[pl.ds(0, plane - 1)]
     remote(rest, rest, at["a3"], other).wait_recv()
+    for p in range(plane):
+        stage[p * per:(p + 1) * per, :] = ag_a[p].astype(F32)
     for b in range(blocks):
         for j in range(taps + 2):
             row = b * (taps + 2) + j
-            v = ag_a[row // per, row % per:row % per + 1, :]
+            v = stage[row:row + 1, :]
             if j < taps:
                 taps_o[j:j + 1, lanes(b)] = v
             else:
@@ -609,8 +617,8 @@
         vm((2, nz, 16, third), BF16), vm((2, nz - 1, 16, third), BF16),
         vm((nx, ny, 16, third), BF16), vm((nx - 1, ny, 16, third), BF16),
         vm((ny, 16, third), BF16), vm((ny - 1, 16, third), BF16),
-        vm((plane * per, LANE), F32), vm((plane, per, LANE), BF16), vm((plane - 1, per, LANE), BF16), vm((per, LANE), F32),
-        vm((nz, per, LANE), F32), vm((per, LANE), F32), vm((plane, per, LANE), F32),
+        vm((plane * per, LANE), F32), vm((plane, per, LANE), BF16), vm((plane - 1, per, LANE), BF16), vm((per, LANE), BF16),
+        vm((nz, per, LANE), BF16), vm((per, LANE), BF16), vm((plane, per, LANE), BF16),
         pltpu.SemaphoreType.DMA((8,)),
         pltpu.SemaphoreType.DMA((slots.used,)), pltpu.SemaphoreType.DMA((slots.used,)),
     ]

time: 42.3 us -> 41.5 us (0.981)
  Pallas kernels: 41.5 us -> 40.8 us
    pallas_call x1, Pallas kernels: 40.3 us -> 39.6 us  [local(): pl.pallas_call(functools.partial(kernel, (nz, ny, nx, rows, chan, depth,...]
where the time goes in v4:
time: 41.5 us; the launch traced here: 41.4 us
  Pallas kernels  40.8 us (98%)
  between operations  0.64 us (2%)
    pallas_call x1, Pallas kernels, local(): pl.pallas_call(functools.partial(kernel, (nz, ny, nx, rows, chan, depth,...  39.6 us
    pallas_call x1, Pallas kernels, local(): pl.pallas_call(write_out, out_shape=tuple((jax.ShapeDtypeStruct(*s) for s...  1.23 us

profile of v4, /device:TPU:2, one launch (start us, length us, event | category | flops | bytes accessed | tf_op | source)
XLA Modules:
  0.0 41.4 jit_solution(8779845490701182260)
XLA Ops:
  0.6 39.6 %module_backward.1 = (bf16[512,768]{1,0:T(8,128)(2,1)S(1)}, bf16[512,768]{1,0:T(8,128)(2,1)S(1)}, f32[31,768]{1,0:T(8,128)S(1)}, f32[768]{0:T(1024)S(1)}, f32[768]{0:T(1024)S(1)}, /*index=5*/f32[16,768]{1,0:T(8,128)S(1)}) custom-call(bf16[512,768]{1,0:T(8,128)(2,1)} %refs_0_.1, bf16[512,768]{1,0:T(8,128)(2,1)} %refs_1_.1, bf16[512,768]{1,0:T(8,128)(2,1)} %refs_2_.1, ...), custom_call_target="tpu_custom_call" | custom-call | tf_op jit(solution)/shard_map/module_backward/pallas_call | solution.py:630
  40.2 1.2 %write_out.1 = (bf16[512,768]{1,0:T(8,128)(2,1)}, bf16[512,768]{1,0:T(8,128)(2,1)}, f32[31,768]{1,0:T(8,128)}, f32[768]{0:T(1024)}, f32[768]{0:T(1024)}, /*index=5*/f32[16,768]{1,0:T(8,128)}) custom-call(bf16[512,768]{1,0:T(8,128)(2,1)S(1)} %get-tuple-element.12.refs_0_, bf16[512,768]{1,0:T(8,128)(2,1)S(1)} %get-tuple-element.13.refs_1_, ...), custom_call_target="tpu_custom_call" | custom-call | tf_op jit(solution)/shard_map/write_out/pallas_call | solution.py:641

commit v5 on v4

--- a/solution.py
+++ b/solution.py
@@ -249,6 +249,12 @@
     def ring_wait(step, leads):
         return remote(pz.at[0], pz.at[0], at["leads" if leads else "trails"] + step, other)
 
+    def send(stretch, kind):
+        lo, hi = stretches[stretch]
+        for axis in ("x", "y"):
+            for direction in (1, -1):
+                hop(axis, stretch, kind, direction, pl.ds(lo, hi - lo)).start()
+
     def project(stretch):
         def step(i, carry):
             lines = pl.ds(pl.multiple_of(i * 2 * span, span), 2 * span)
@@ -278,10 +284,7 @@
 
         lo, hi = stretches[stretch]
         lax.fori_loop(lo // 2, hi // 2, step, 0)
-        for kind in (FAR, NEAR):
-            for axis in ("x", "y"):
-                for direction in (1, -1):
-                    hop(axis, stretch, kind, direction, pl.ds(lo, hi - lo)).start()
+        send(stretch, FAR)
 
     def z_step(step, leads):
         ring_wait(step - 1, leads).wait_recv()
@@ -293,6 +296,7 @@
             ring(step, leads, dest, direction).start()
 
     project(0)
+    send(0, NEAR)
 
     ag_v[FIRST:, :] = jnp.dot(og_v[FIRST:, :], w_v[...], preferred_element_type=F32)
 
@@ -333,6 +337,7 @@
 
     project(1)
     relay(0)
+    send(1, NEAR)
     z_step(1, True)
 
     @pl.when(line > 0)

time: 41.5 us -> 41.8 us (level)
  no operation moved by 1% of the time
where the time goes in v5:
time: 41.8 us
  Pallas kernels  41.1 us (98%)
  between operations  0.64 us (2%)
    pallas_call x1, Pallas kernels, local(): pl.pallas_call(functools.partial(kernel, (nz, ny, nx, rows, chan, depth,...  39.9 us
    pallas_call x1, Pallas kernels, local(): pl.pallas_call(write_out, out_shape=tuple((jax.ShapeDtypeStruct(*s) for s...  1.23 us

profile of v5, /device:TPU:2, one launch (start us, length us, event | category | flops | bytes accessed | tf_op | source)
XLA Modules:
  0.0 41.8 jit_solution(1719082580098438562)
XLA Ops:
  0.6 39.9 %module_backward.1 = (bf16[512,768]{1,0:T(8,128)(2,1)S(1)}, bf16[512,768]{1,0:T(8,128)(2,1)S(1)}, f32[31,768]{1,0:T(8,128)S(1)}, f32[768]{0:T(1024)S(1)}, f32[768]{0:T(1024)S(1)}, /*index=5*/f32[16,768]{1,0:T(8,128)S(1)}) custom-call(bf16[512,768]{1,0:T(8,128)(2,1)} %refs_0_.1, bf16[512,768]{1,0:T(8,128)(2,1)} %refs_1_.1, bf16[512,768]{1,0:T(8,128)(2,1)} %refs_2_.1, ...), custom_call_target="tpu_custom_call" | custom-call | tf_op jit(solution)/shard_map/module_backward/pallas_call | solution.py:635
  40.5 1.2 %write_out.1 = (bf16[512,768]{1,0:T(8,128)(2,1)}, bf16[512,768]{1,0:T(8,128)(2,1)}, f32[31,768]{1,0:T(8,128)}, f32[768]{0:T(1024)}, f32[768]{0:T(1024)}, /*index=5*/f32[16,768]{1,0:T(8,128)}) custom-call(bf16[512,768]{1,0:T(8,128)(2,1)S(1)} %get-tuple-element.12.refs_0_, bf16[512,768]{1,0:T(8,128)(2,1)S(1)} %get-tuple-element.13.refs_1_, ...), custom_call_target="tpu_custom_call" | custom-call | tf_op jit(solution)/shard_map/write_out/pallas_call | solution.py:646
